TPU v7x, 256 devices: a whole 4x4x8 slice. The times are simulated.
256 devices in a mesh: fs: 32 (over z, y), tp: 8 (over x, core).
Axes of the slice: x: 4, y: 4, z: 8, core: 2. Of those that a mesh axis runs over, the one named last changes fastest.
Arguments:
- prompt: bfloat16 [32768, 2048], P(('fs', 'tp')), may hold values from -6 to 6
- norm_gain: float32 [2048], P('fs'), may hold values from 0.1 to 1.9
- up_trained: float32 [2048, 8192], P('fs', 'tp'), may hold values from -0.125 to 0.125
- down_trained: float32 [2048, 8192], P('fs', 'tp'), may hold values from -0.0625 to 0.0625
Outputs:
- up_served: bfloat16 [2048, 8192], P(None, 'tp')
- down_served: bfloat16 [8192, 2048], P('tp')
- mixed: bfloat16 [32768, 2048], P(('fs', 'tp'))
All inputs are finite; a program needn't handle non-finite values.
Results may differ from a plain program's by a relative error of at most 0.014.
Values may be sent and summed in bfloat16 or wider, within the bound.
No kernel may reach another device: no remote copies, remote signals or barrier semaphores. Data moves between devices by JAX's collectives and lax.ppermute only.
A program may use at most 128 MiB of HBM per device.

v0:
```python
import jax
import jax.numpy as jnp
from jax import lax
from jax.sharding import PartitionSpec as P


def sent_together(arrays, axis, dim, along):
    both = jnp.concatenate(arrays, axis=along)
    filled, at, finished = (lax.all_gather(both, axis, axis=dim, tiled=True), 0, [])
    for a in arrays:
        finished.append(lax.slice_in_dim(filled, at, at + a.shape[along], axis=along))
        at += a.shape[along]
    return tuple(finished)


def shards(prompt, norm_gain, up_trained, down_trained):
    up_local = (norm_gain[:, None] * up_trained).astype(jnp.bfloat16)
    down_local = down_trained.astype(jnp.bfloat16)
    values = prompt.astype(jnp.float32)
    scale = lax.rsqrt(jnp.mean(values * values, axis=-1, keepdims=True) + 1e-06)
    normed = (values * scale).astype(jnp.bfloat16)
    group_rows = lax.all_gather(normed, "tp", axis=0, tiled=True)
    up_whole, down_whole = sent_together((up_local, down_local), "fs", 0, 1)
    pre = jnp.dot(group_rows, up_whole, preferred_element_type=jnp.float32)
    hidden = jnp.square(jax.nn.relu(pre)).astype(jnp.bfloat16)
    down_served = jnp.transpose(down_whole)
    mixed = lax.psum_scatter(
        jnp.dot(hidden, down_served, preferred_element_type=jnp.float32).astype(jnp.bfloat16),
        "tp",
        scatter_dimension=0,
        tiled=True,
    )
    return (up_whole, down_served, mixed)


def solution(mesh):
    return jax.shard_map(
        shards,
        mesh=mesh,
        in_specs=(P(("fs", "tp"), None), P("fs"), P("fs", "tp"), P("fs", "tp")),
        out_specs=(P(None, "tp"), P("tp", None), P(("fs", "tp"), None)),
        check_vma=False,
    )
```

profile of v0, /device:TPU:8, one launch (start us, length us, event | category | flops | bytes accessed | tf_op | source)
XLA Modules:
  0.0 207.6 jit_solution(5565873400041753207)
XLA Ops:
  7.2 0.0 all-gather.3.cloned.1.call-start
  7.2 1.0 convert_element_type.19
  8.2 1.0 multiply_convert_fusion.1
  9.2 0.7 pad_maximum_fusion
  9.9 0.0 all-gather.3.cloned.1.call-update
  10.0 0.0 all-gather.5.cloned.1.call-start
  10.0 1.2 fusion.1
  11.3 2.0 fusion.2
  13.2 0.0 all-gather.5.cloned.1.call-update
  13.3 0.0 reduce-scatter.2.cloned.1.call-start
  13.3 97.3 %all-gather.3.cloned.1.call-done = bf16[2048,2048]{1,0:T(8,128)(2,1)} async-done(((bf16[64,2048]{1,0:T(8,128)(2,1)}), bf16[2048,2048]{1,0:T(8,128)(2,1)}) %all-gather.3.cloned.1.call-update) | async-done | bytes 8388624 | tf_op jit(solution)/shard_map/all_gather | solution.py:9
  110.7 6.0 %slice_bitcast_fusion = (bf16[1024,2048]{0,1:T(8,128)(2,1)}, bf16[2048,1024]{1,0:T(8,128)(2,1)}) fusion(bf16[2048,2048]{1,0:T(8,128)(2,1)} %all-gather.3.cloned.1.call-done), kind=kLoop, calls=%fused_computation.3 | loop fusion | bytes 16777216 | tf_op jit(solution)/shard_map/transpose | solution.py:26
  116.7 29.4 %all-gather.5.cloned.1.call-done = bf16[1024,2048]{1,0:T(8,128)(2,1)} async-done(((bf16[128,2048]{1,0:T(8,128)(2,1)}), bf16[1024,2048]{1,0:T(8,128)(2,1)}) %all-gather.5.cloned.1.call-update) | async-done | bytes 4194320 | tf_op jit(solution)/shard_map/all_gather | solution.py:22
  146.0 14.4 %convolution_convert_fusion = bf16[1024,2048]{1,0:T(8,128)(2,1)} fusion(bf16[2048,2048]{1,0:T(8,128)(2,1)} %all-gather.3.cloned.1.call-done, bf16[1024,2048]{1,0:T(8,128)(2,1)} %all-gather.5.cloned.1.call-done, bf16[2048,1024]{1,0:T(8,128)(2,1)} %get-tuple-element.10), kind=kOutput, calls=%fused_computation.1 | convolution fusion | flops 8595177472 | bytes 16777216 | tf_op jit(solution)/shard_map/dot_general | solution.py:28
  160.4 0.0 reduce-scatter.2.cloned.1.call-update
  160.4 6.4 %copy.10 = bf16[1024,2048]{1,0:T(8,128)(2,1)} copy(bf16[1024,2048]{0,1:T(8,128)(2,1)} %get-tuple-element.9) | data formatting | bytes 8388608
  166.9 34.2 %reduce-scatter.2.cloned.1.call-done = bf16[128,2048]{1,0:T(8,128)(2,1)} async-done(((bf16[1024,2048]{1,0:T(8,128)(2,1)}), bf16[128,2048]{1,0:T(8,128)(2,1)}) %reduce-scatter.2.cloned.1.call-update) | async-done | bytes 524304 | tf_op jit(solution)/shard_map/reduce_scatter | solution.py:27
  (1 shorter events, 0.0 us)
Async XLA Ops:
  7.2 103.5 %all-gather.3.cloned.1.call-start = ((), (), s32[]{:S(2)}) async-start(), calls=%async_computation.1 | async-start | bytes 8650752 | tf_op jit(solution)/shard_map/all_gather | solution.py:9
  10.0 136.1 %all-gather.5.cloned.1.call-start = ((), (), s32[]{:S(2)}) async-start(), calls=%async_computation.2 | async-start | bytes 4718592 | tf_op jit(solution)/shard_map/all_gather | solution.py:22
  13.3 187.8 %reduce-scatter.2.cloned.1.call-start = ((), (), s32[]{:S(2)}) async-start(), calls=%async_computation.3 | async-start | bytes 4718592 | tf_op jit(solution)/shard_map/reduce_scatter | solution.py:27
Sparse Core Ops, SparseCore 0:
  11.1 99.4 all-gather.2
  113.1 32.8 all-gather.4
  160.5 40.4 reduce-scatter.1
where the time goes:
time: 208 us
  waiting for transfers between devices  161 us (77%)
  matrix products  14.4 us (7%)
  between operations  13.8 us (7%)
  local copies, waits for them, and re-layouts  12.5 us (6%)
  other arithmetic  5.96 us (3%)
    all_gather x1, waiting for transfers between devices, sent_together(): lax.all_gather(both, axis, axis=dim, tiled=True)  97.3 us
    reduce_scatter x1, waiting for transfers between devices, shards(): lax.psum_scatter(jnp.dot(hidden, down_served, preferred_element_type=jnp....  34.2 us
    all_gather x1, waiting for transfers between devices, shards(): group_rows = lax.all_gather(normed, 'tp', axis=0, tiled=True)  29.4 us
    dot_general x1, matrix products, shards(): jnp.dot(hidden, down_served, preferred_element_type=jnp.float32)  14.4 us
    unnamed x1, local copies, waits for them, and re-layouts  6.43 us
    transpose x1, local copies, waits for them, and re-layouts, shards(): down_served = jnp.transpose(down_whole)  6.02 us
  transfers between devices with their start and end apart: 3, of which 3 were waited for; matrix products, arithmetic and copies ran while one was open for 8% of the time, Pallas kernels for 0%

commit v1 on v0

v1 whole, which is shorter than its diff:
```python
import functools

import jax
import jax.numpy as jnp
from jax import lax
from jax.experimental import pallas as pl
from jax.experimental.pallas import tpu as pltpu
from jax.sharding import PartitionSpec as P


NZ, NY, NX, NC = 8, 4, 4, 2
VMEM = pl.BlockSpec(memory_space=pltpu.VMEM)
ANY = pl.BlockSpec(memory_space=pl.ANY)
GROUPS = ((0, 1, -1, 2, -2), (3, -3, 4))
CHUNKS = ((0, 0, 2), (0, 2, 3), (1, 0, 3))
NEAR, MID = (-2, -1, 0, 1, 2), (-3, 3)


def rot(v, axis, n, by):
    return lax.ppermute(v, axis, [(i, (i + by) % n) for i in range(n)])


def limit(mib):
    return pltpu.CompilerParams(vmem_limit_bytes=mib * 2**20)


def cost(flops, nbytes):
    return pl.CostEstimate(flops=flops, bytes_accessed=nbytes, transcendentals=0)


def row_of(dz):
    return lax.rem(lax.axis_index("z") + (dz + NZ), NZ) * 256


def norm_kernel(x_ref, o_ref):
    x = x_ref[...].astype(jnp.float32)
    scale = lax.rsqrt(jnp.mean(x * x, axis=-1, keepdims=True) + 1e-06)
    for i in range(NZ):
        block = x_ref[:, pl.ds(pl.multiple_of(row_of(i - 3), 256), 256)].astype(jnp.float32)
        o_ref[:, i * 256 : (i + 1) * 256] = (block * scale).astype(o_ref.dtype)


def norm(x):
    return pl.pallas_call(
        norm_kernel,
        out_shape=jax.ShapeDtypeStruct(x.shape, jnp.bfloat16),
        in_specs=[VMEM],
        out_specs=VMEM,
        compiler_params=limit(8),
        name="norm",
    )(x)


def place_kernel(spots, cut, *refs):
    sem, o_ref, parts = refs[-1], refs[-2], refs[:-2]
    copies = []
    for n, (part, (spot, left)) in enumerate(zip(parts, spots)):
        rows = part.shape[0]
        at = pl.multiple_of(spot(), rows) if callable(spot) else spot
        wide = part.shape[1]
        if cut is not None:
            part, wide = part.at[:, cut[0] : cut[1]], cut[1] - cut[0]
        to = o_ref.at[pl.ds(at, rows), left : left + wide]
        copies.append(pltpu.make_async_copy(part, to, sem.at[n]))
        copies[-1].start()
    for c in copies:
        c.wait()


def place(parts, spots, shape, out, cut=None):
    return pl.pallas_call(
        functools.partial(place_kernel, spots, cut),
        out_shape=jax.ShapeDtypeStruct(shape, jnp.bfloat16),
        in_specs=[ANY] * len(parts),
        out_specs=out,
        scratch_shapes=[pltpu.SemaphoreType.DMA((len(parts),))],
        compiler_params=limit(8),
        name="place",
    )(*parts)


def up_kernel(n, more, last, *refs):
    own, oth, parts, o_ref = refs[:n], refs[n : 2 * n], refs[2 * n : 3 * n], refs[-1]
    half = own[0].shape[0]
    rhs = jnp.concatenate([p[...] for p in parts], axis=0)
    for c, group in enumerate((own, oth)):
        lhs = jnp.concatenate([t[...] for t in group], axis=1)
        dot = jnp.dot(lhs, rhs, preferred_element_type=jnp.float32)
        if more:
            dot = dot + refs[3 * n][c * half : (c + 1) * half, :]
        if last:
            dot = jnp.square(jnp.maximum(dot, 0.0))
        o_ref[c * half : (c + 1) * half, :] = dot.astype(o_ref.dtype)


def up_dot(own, oth, parts, acc=None, last=False):
    more, n = acc is not None, len(parts)
    rows, wide, tile = own.shape[0], parts[0][0].shape[1], 256
    tokens, pieces, depth = [], [], 0
    for p, at in parts:
        k = p.shape[0]
        tokens.append(pl.BlockSpec((rows, k), lambda j, i=at // k: (0, i)))
        pieces.append(pl.BlockSpec((k, tile), lambda j: (0, j)))
        depth += k
    col = pl.BlockSpec((2 * rows, tile), lambda j: (0, j))
    return pl.pallas_call(
        functools.partial(up_kernel, n, more, last),
        grid=(wide // tile,),
        out_shape=jax.ShapeDtypeStruct((2 * rows, wide), jnp.bfloat16 if last else jnp.float32),
        in_specs=tokens * 2 + pieces + ([col] if more else []),
        out_specs=col,
        compiler_params=limit(24),
        cost_estimate=cost(4 * rows * wide * depth, 6 * 2**20),
        name="up",
    )(*[own] * n, *[oth] * n, *[p for p, _ in parts], *((acc,) if more else ()))


def down_kernel(first, h_ref, a_ref, b_ref, c_ref, d_ref, own_ref, oth_ref):
    half = h_ref.shape[0] // 2
    rows = pl.ds(pl.multiple_of((pl.program_id(0) + first) * 64, 64), 64)
    rhs = jnp.concatenate([r[rows, :] for r in (a_ref, b_ref, c_ref, d_ref)], axis=0)
    for c, o_ref in enumerate((own_ref, oth_ref)):
        cut = slice(c * half, (c + 1) * half)
        o_ref[...] = lax.dot_general(
            h_ref[cut, :], rhs, (((1,), (1,)), ((), ())), preferred_element_type=jnp.float32
        ).astype(o_ref.dtype)


def down_dot(hidden, parts, first, n):
    rows, k = parts[0].shape
    m, wide = hidden.shape
    out = jax.ShapeDtypeStruct((m // 2, n * 256), jnp.bfloat16)
    col = pl.BlockSpec((m // 2, 256), lambda j: (0, j))
    return pl.pallas_call(
        functools.partial(down_kernel, first),
        grid=(n,),
        out_shape=(out, out),
        in_specs=[pl.BlockSpec((m, wide), lambda j: (0, 0))]
        + [pl.BlockSpec((rows, k), lambda j: (0, 0))] * NY,
        out_specs=(col, col),
        compiler_params=limit(24),
        cost_estimate=cost(2 * m * k * 256 * n, 6 * 2**20),
        name="down",
    )(hidden, *parts)


def turn_kernel(*refs):
    o_ref, block, out, sem = refs[-4:]
    y = lax.axis_index("y")

    def copy(seen):
        dz = jnp.where(lax.rem(seen, 2) == 1, (seen + 1) // 2, -(seen // 2))
        at = pl.multiple_of(row_of(dz), 256)
        return pltpu.make_async_copy(out.at[seen], o_ref.at[:, pl.ds(at, 256)], sem.at[seen])

    base = 0
    for g, dzs in enumerate(GROUPS):

        @pl.loop(0, len(dzs))
        def _(j, g=g, base=base):
            for k in range(NY):
                rows = pl.ds(pl.multiple_of(j * 64, 64), 64)
                block[lax.rem(y + k, NY)] = refs[4 * g + k][rows, :]
            out[base + j] = block[...].reshape(256, block.shape[2]).T
            copy(base + j).start()

        base += len(dzs)

    @pl.loop(0, NZ)
    def _(j):
        copy(j).wait()


def turn(parts):
    cols = parts[0].shape[1]
    return pl.pallas_call(
        turn_kernel,
        out_shape=jax.ShapeDtypeStruct((cols, NZ * 256), jnp.bfloat16),
        in_specs=[VMEM] * len(parts),
        out_specs=ANY,
        scratch_shapes=[
            pltpu.VMEM((NY, 64, cols), jnp.bfloat16),
            pltpu.VMEM((NZ, cols, 256), jnp.bfloat16),
            pltpu.SemaphoreType.DMA((NZ,)),
        ],
        compiler_params=limit(16),
        cost_estimate=cost(2 * 10**9, 8 * 2**20),
        name="turn",
    )(*parts)


def total_kernel(*refs):
    o_ref = refs[-1]
    shift = lax.axis_index("y") * 64
    for g, (at, first, n) in enumerate(CHUNKS):
        for j in range(n):
            cut = slice(j * 256, (j + 1) * 256)
            a, b, c, d = (r[:, cut].astype(jnp.float32) for r in refs[4 * g : 4 * g + 4])
            s = pltpu.roll((a + b) + (c + d), shift, 1)
            to = pl.ds(pl.multiple_of(row_of(GROUPS[at][first + j]), 256), 256)
            o_ref[:, to] = s.astype(o_ref.dtype)


def total(parts):
    return pl.pallas_call(
        total_kernel,
        out_shape=jax.ShapeDtypeStruct((parts[0].shape[0], NZ * 256), jnp.bfloat16),
        in_specs=[VMEM] * len(parts),
        out_specs=VMEM,
        compiler_params=limit(8),
        name="total",
    )(*parts)


def layer(prompt, norm_gain, up_trained, down_trained):
    up = (norm_gain[:, None] * up_trained).astype(jnp.bfloat16)
    down = down_trained.astype(jnp.bfloat16)

    def by_y(k):
        return lambda: lax.rem(lax.axis_index("y") + k, NY) * 64

    parts = (up, rot(up, "y", NY, -1), rot(up, "y", NY, 2), rot(up, "y", NY, 1))
    spots = [(by_y(k), 0) for k in range(NY)]
    wide = up.shape[1]
    ups = {0: place(parts, spots, (256, wide), VMEM)}

    normed = norm(prompt)
    parts = (normed, rot(normed, "x", NX, -1), rot(normed, "x", NX, 2), rot(normed, "x", NX, 1))
    own = place(parts, [(128 * k, 0) for k in range(NX)], (512, NZ * 256), VMEM)
    oth = rot(own, "c", NC, 1)

    downs = {0: down}
    for k in (1, 2, 3):
        ups[k] = rot(ups[k - 1], "z", NZ, -1)
        ups[-k] = rot(ups[1 - k], "z", NZ, 1)
        frm, hops = (0, k) if k < 3 else (2, 1)
        downs[k] = rot(downs[frm], "z", NZ, -hops)
        downs[-k] = rot(downs[-frm], "z", NZ, hops)
    far = (rot(ups[3][:128], "z", NZ, -1), rot(ups[-3][128:], "z", NZ, 1))
    downs[4] = rot(downs[3], "z", NZ, -1)

    parted = []
    for dzs in GROUPS:
        mine = jnp.concatenate([downs[dz] for dz in dzs])
        parted.append((mine, rot(mine, "y", NY, -1), rot(mine, "y", NY, 2), rot(mine, "y", NY, 1)))

    acc = up_dot(own, oth, [(ups[dz], (dz + 3) * 256) for dz in NEAR])
    acc = up_dot(own, oth, [(ups[dz], (dz + 3) * 256) for dz in MID], acc)
    hidden = up_dot(own, oth, [(far[0], 7 * 256), (far[1], 7 * 256 + 128)], acc, last=True)

    summed = []
    for at, first, n in CHUNKS:
        mine, theirs = down_dot(hidden, parted[at], first, n)
        got = rot(theirs, "c", NC, 1)
        s = (mine.astype(jnp.float32) + got.astype(jnp.float32)).astype(jnp.bfloat16)
        summed += [
            s[:128],
            rot(s[128:256], "x", NX, 1),
            rot(s[256:384], "x", NX, 2),
            rot(s[384:], "x", NX, -1),
        ]
    mixed = total(summed)
    down_served = turn([p for parts in parted for p in parts])
    parts = [ups[dz] for dz in NEAR + MID] + list(far)
    spots = [(functools.partial(row_of, dz), 0) for dz in NEAR + MID]
    spots += [(functools.partial(row_of, 4), 0), (lambda: row_of(4) + 128, 0)]
    up_served = place(parts, spots, (NZ * 256, wide), ANY)
    return up_served, down_served, mixed


def solution(mesh):
    grid = jax.sharding.Mesh(mesh.devices.reshape(NZ, NY, NX, NC), ("z", "y", "x", "c"))
    fs, tp = ("z", "y"), ("x", "c")
    return jax.shard_map(
        layer,
        mesh=grid,
        in_specs=(P(fs + tp, None), P(fs), P(fs, tp), P(fs, tp)),
        out_specs=(P(None, tp), P(tp, None), P(fs + tp, None)),
        check_vma=False,
    )
```

time: 208 us -> 174 us (0.84)
  waiting for transfers between devices: 161 us -> 91.6 us
  starting transfers between devices: 0.12 us -> 55.8 us
  Pallas kernels: 0 us -> 23.1 us
  matrix products: 14.4 us -> 0 us
  between operations: 13.8 us -> 0.94 us
  local copies, waits for them, and re-layouts: 12.5 us -> 1.29 us
  other arithmetic: 5.96 us -> 1.55 us
    all_gather x2 -> x0, waiting for transfers between devices: 127 us -> none  [the longest x1 97.3 us: sent_together(): lax.all_gather(both, axis, axis=dim, tiled=True)]
    ppermute x0 -> x40, waiting for transfers between devices: none -> 91.6 us  [rot(): return lax.ppermute(v, axis, [(i, (i + by) % n) for i in range(n)])]
    ppermute x0 -> x40, starting transfers between devices: none -> 55.8 us  [rot(): return lax.ppermute(v, axis, [(i, (i + by) % n) for i in range(n)])]
    reduce_scatter x1 -> x0, waiting for transfers between devices: 34.2 us -> none  [shards(): lax.psum_scatter(jnp.dot(hidden, down_served, preferred_element_type=jnp....]
    pallas_call x0 -> x12, Pallas kernels: none -> 23.1 us  [the longest x3 9.49 us: up_dot(): pl.pallas_call(functools.partial(up_kernel, n, more, last), grid=(wide //...]
    dot_general x1 -> x0, matrix products: 14.4 us -> none  [shards(): jnp.dot(hidden, down_served, preferred_element_type=jnp.float32)]
    transpose x1 -> x0, local copies, waits for them, and re-layouts: 6.02 us -> none  [shards(): down_served = jnp.transpose(down_whole)]
    unnamed x1 -> x9, local copies, waits for them, and re-layouts: 6.43 us -> 1.09 us
  transfers between devices with their start and end apart: 3 -> 40, of which waited for: 3 -> 18; matrix products, arithmetic and copies ran while one was open for 8% -> 1% of each run, Pallas kernels for 0% -> 12%
where the time goes in v1:
time: 174 us
  waiting for transfers between devices  91.6 us (53%)
  starting transfers between devices  55.8 us (32%)
  Pallas kernels  23.1 us (13%)
    ppermute x40, waiting for transfers between devices, rot(): return lax.ppermute(v, axis, [(i, (i + by) % n) for i in range(n)])  91.6 us
    ppermute x40, starting transfers between devices, rot(): return lax.ppermute(v, axis, [(i, (i + by) % n) for i in range(n)])  55.8 us
    pallas_call x3, Pallas kernels, up_dot(): pl.pallas_call(functools.partial(up_kernel, n, more, last), grid=(wide //...  9.49 us
    pallas_call x3, Pallas kernels, down_dot(): pl.pallas_call(functools.partial(down_kernel, first), grid=(n,), out_shap...  6.28 us
  transfers between devices with their start and end apart: 40, of which 18 were waited for; matrix products, arithmetic and copies ran while one was open for 1% of the time, Pallas kernels for 12%

profile of v1, /device:TPU:8, one launch (start us, length us, event | category | flops | bytes accessed | tf_op | source)
XLA Modules:
  0.0 174.2 jit_solution(14543077579383257492)
XLA Ops:
  0.6 1.0 copy-done
  1.9 2.8 %collective-permute-start.24 = (bf16[128,2048]{1,0:T(8,128)(2,1)S(1)}, bf16[128,2048]{1,0:T(8,128)(2,1)S(1)}, u32[]{:S(2)}, u32[]{:S(2)}) collective-permute-start(bf16[128,2048]{1,0:T(8,128)(2,1)S(1)} %norm.1.refs_0_), channel_id=1, source_target_pairs={{0,6},{2,0},{4,2},{6,4},{1,7},{3,1},{5,3},{7,5},{8,14},{10,8},{12,... | collective-permute-start | bytes 1572872 | tf_op jit(solution)/shard_map/ppermute | solution.py:20
  6.4 1.0 multiply_convert_fusion.refs_0_
  8.0 2.6 %collective-permute-start.1 = (bf16[64,1024]{1,0:T(8,128)(2,1)S(1)}, bf16[64,1024]{1,0:T(8,128)(2,1)S(1)}, u32[]{:S(2)}, u32[]{:S(2)}) collective-permute-start(bf16[64,1024]{1,0:T(8,128)(2,1)S(1)} %multiply_convert_fusion.refs_0_), channel_id=1, source_target_pairs={{0,16},{8,24},{16,0},{24,8},{1,17},{9,25},{17,1},{25,9},{2,18},{10... | collective-permute-start | bytes 393224 | tf_op jit(solution)/shard_map/ppermute | solution.py:20
  10.6 3.3 %collective-permute-done.refs_1_ = bf16[64,1024]{1,0:T(8,128)(2,1)S(1)} collective-permute-done((bf16[64,1024]{1,0:T(8,128)(2,1)S(1)}, bf16[64,1024]{1,0:T(8,128)(2,1)S(1)}, u32[]{:S(2)}, u32[]{:S(2)}) %collective-permute-start) | collective-permute-done | bytes 131104 | tf_op jit(solution)/shard_map/ppermute | solution.py:20
  13.9 1.0 collective-permute-start.2
  15.7 3.1 %collective-permute-done.2.refs_3_ = bf16[64,1024]{1,0:T(8,128)(2,1)S(1)} collective-permute-done((bf16[64,1024]{1,0:T(8,128)(2,1)S(1)}, bf16[64,1024]{1,0:T(8,128)(2,1)S(1)}, u32[]{:S(2)}, u32[]{:S(2)}) %collective-permute-start.2) | collective-permute-done | bytes 131104 | tf_op jit(solution)/shard_map/ppermute | solution.py:20
  19.6 2.0 %collective-permute-start.3 = (bf16[256,1024]{1,0:T(8,128)(2,1)S(1)}, bf16[256,1024]{1,0:T(8,128)(2,1)S(1)}, u32[]{:S(2)}, u32[]{:S(2)}) collective-permute-start(bf16[256,1024]{1,0:T(8,128)(2,1)S(1)} %place.3.refs_2_.refs_12_), channel_id=1, source_target_pairs={{0,32},{32,64},{64,96},{96,128},{128,160},{160,192},{192,224},{224... | collective-permute-start | bytes 1572872 | tf_op jit(solution)/shard_map/ppermute | solution.py:20
  21.6 5.6 %collective-permute-done.24.refs_1_ = bf16[128,2048]{1,0:T(8,128)(2,1)S(1)} collective-permute-done((bf16[128,2048]{1,0:T(8,128)(2,1)S(1)}, bf16[128,2048]{1,0:T(8,128)(2,1)S(1)}, u32[]{:S(2)}, u32[]{:S(2)}) %collective-permute-start.24) | collective-permute-done | bytes 524320 | tf_op jit(solution)/shard_map/ppermute | solution.py:20
  27.2 3.7 %collective-permute-done.26.refs_3_ = bf16[128,2048]{1,0:T(8,128)(2,1)S(1)} collective-permute-done((bf16[128,2048]{1,0:T(8,128)(2,1)S(1)}, bf16[128,2048]{1,0:T(8,128)(2,1)S(1)}, u32[]{:S(2)}, u32[]{:S(2)}) %collective-permute-start.26) | collective-permute-done | bytes 524320 | tf_op jit(solution)/shard_map/ppermute | solution.py:20
  31.1 5.9 %collective-permute-start.5 = (bf16[256,1024]{1,0:T(8,128)(2,1)S(1)}, bf16[256,1024]{1,0:T(8,128)(2,1)S(1)}, u32[]{:S(2)}, u32[]{:S(2)}) collective-permute-start(bf16[256,1024]{1,0:T(8,128)(2,1)S(1)} %place.3.refs_2_.refs_12_), channel_id=1, source_target_pairs={{0,224},{32,0},{64,32},{96,64},{128,96},{160,128},{192,160},{224,1... | collective-permute-start | bytes 1572872 | tf_op jit(solution)/shard_map/ppermute | solution.py:20
  37.1 3.3 %collective-permute-start.11 = (bf16[64,1024]{1,0:T(8,128)(2,1)S(1)}, bf16[64,1024]{1,0:T(8,128)(2,1)S(1)}, u32[]{:S(2)}, u32[]{:S(2)}) collective-permute-start(bf16[64,1024]{1,0:T(8,128)(2,1)S(1)} %get-tuple-element.16), channel_id=1, source_target_pairs={{0,224},{32,0},{64,32},{96,64},{128,96},{160,128},{192,160},{224,1... | collective-permute-start | bytes 393224 | tf_op jit(solution)/shard_map/ppermute | solution.py:20
  40.4 11.2 %collective-permute-done.11 = bf16[64,1024]{1,0:T(8,128)(2,1)S(1)} collective-permute-done((bf16[64,1024]{1,0:T(8,128)(2,1)S(1)}, bf16[64,1024]{1,0:T(8,128)(2,1)S(1)}, u32[]{:S(2)}, u32[]{:S(2)}) %collective-permute-start.11) | collective-permute-done | bytes 131104 | tf_op jit(solution)/shard_map/ppermute | solution.py:20
  51.6 2.9 %collective-permute-start.13 = (bf16[64,1024]{1,0:T(8,128)(2,1)S(1)}, bf16[64,1024]{1,0:T(8,128)(2,1)S(1)}, u32[]{:S(2)}, u32[]{:S(2)}) collective-permute-start(bf16[64,1024]{1,0:T(8,128)(2,1)S(1)} %get-tuple-element.16), channel_id=1, source_target_pairs={{0,192},{32,224},{64,0},{96,32},{128,64},{160,96},{192,128},{224,1... | collective-permute-start | bytes 393224 | tf_op jit(solution)/shard_map/ppermute | solution.py:20
  54.6 1.0 collective-permute-start.6
  55.6 2.8 %collective-permute-start.14 = (bf16[64,1024]{1,0:T(8,128)(2,1)S(1)}, bf16[64,1024]{1,0:T(8,128)(2,1)S(1)}, u32[]{:S(2)}, u32[]{:S(2)}) collective-permute-start(bf16[64,1024]{1,0:T(8,128)(2,1)S(1)} %get-tuple-element.16), channel_id=1, source_target_pairs={{0,64},{32,96},{64,128},{96,160},{128,192},{160,224},{192,0},{224,... | collective-permute-start | bytes 393224 | tf_op jit(solution)/shard_map/ppermute | solution.py:20
  58.4 2.7 %collective-permute-done.13 = bf16[64,1024]{1,0:T(8,128)(2,1)S(1)} collective-permute-done((bf16[64,1024]{1,0:T(8,128)(2,1)S(1)}, bf16[64,1024]{1,0:T(8,128)(2,1)S(1)}, u32[]{:S(2)}, u32[]{:S(2)}) %collective-permute-start.13) | collective-permute-done | bytes 131104 | tf_op jit(solution)/shard_map/ppermute | solution.py:20
  61.1 1.0 collective-permute-start.7
  62.1 2.2 %collective-permute-done.14 = bf16[64,1024]{1,0:T(8,128)(2,1)S(1)} collective-permute-done((bf16[64,1024]{1,0:T(8,128)(2,1)S(1)}, bf16[64,1024]{1,0:T(8,128)(2,1)S(1)}, u32[]{:S(2)}, u32[]{:S(2)}) %collective-permute-start.14) | collective-permute-done | bytes 131104 | tf_op jit(solution)/shard_map/ppermute | solution.py:20
  65.1 7.5 %collective-permute-done.6.refs_4_.refs_14_ = bf16[256,1024]{1,0:T(8,128)(2,1)S(1)} collective-permute-done((bf16[256,1024]{1,0:T(8,128)(2,1)S(1)}, bf16[256,1024]{1,0:T(8,128)(2,1)S(1)}, u32[]{:S(2)}, u32[]{:S(2)}) %collective-permute-start.6) | collective-permute-done | bytes 524320 | tf_op jit(solution)/shard_map/ppermute | solution.py:20
  72.6 2.2 %collective-permute-start.8 = (bf16[256,1024]{1,0:T(8,128)(2,1)S(1)}, bf16[256,1024]{1,0:T(8,128)(2,1)S(1)}, u32[]{:S(2)}, u32[]{:S(2)}) collective-permute-start(bf16[256,1024]{1,0:T(8,128)(2,1)S(1)} %collective-permute-done.6.refs_4_.refs_14_), channel_id=1, source_target_pairs={{0,224},{32,0},{64,32},{96,64},{128,96},{160,128},{192,160},{224,1... | collective-permute-start | bytes 1572872 | tf_op jit(solution)/shard_map/ppermute | solution.py:20
  74.8 14.3 %collective-permute-done.18 = bf16[64,1024]{1,0:T(8,128)(2,1)S(1)} collective-permute-done((bf16[64,1024]{1,0:T(8,128)(2,1)S(1)}, bf16[64,1024]{1,0:T(8,128)(2,1)S(1)}, u32[]{:S(2)}, u32[]{:S(2)}) %collective-permute-start.18) | collective-permute-done | bytes 131104 | tf_op jit(solution)/shard_map/ppermute | solution.py:20
  89.1 3.2 %collective-permute-start.20 = (bf16[64,1024]{1,0:T(8,128)(2,1)S(1)}, bf16[64,1024]{1,0:T(8,128)(2,1)S(1)}, u32[]{:S(2)}, u32[]{:S(2)}) collective-permute-start(bf16[64,1024]{1,0:T(8,128)(2,1)S(1)} %collective-permute-done.18), channel_id=1, source_target_pairs={{0,224},{32,0},{64,32},{96,64},{128,96},{160,128},{192,160},{224,1... | collective-permute-start | bytes 393224 | tf_op jit(solution)/shard_map/ppermute | solution.py:20
  92.4 2.4 %collective-permute-start.16 = (bf16[320,1024]{1,0:T(8,128)(2,1)S(1)}, bf16[320,1024]{1,0:T(8,128)(2,1)S(1)}, u32[]{:S(2)}, u32[]{:S(2)}) collective-permute-start(bf16[320,1024]{1,0:T(8,128)(2,1)S(1)} %constant_dynamic-update-slice_fusion.refs_0_.a_ref), channel_id=1, source_target_pairs={{0,16},{8,24},{16,0},{24,8},{1,17},{9,25},{17,1},{25,9},{2,18},{10... | collective-permute-start | bytes 1966088 | tf_op jit(solution)/shard_map/ppermute | solution.py:20
  95.3 1.6 collective-permute-start.17
  96.9 3.2 %collective-permute-start.9 = (bf16[128,1024]{1,0:T(8,128)(2,1)S(1)}, bf16[128,1024]{1,0:T(8,128)(2,1)S(1)}, u32[]{:S(2)}, u32[]{:S(2)}) collective-permute-start(bf16[128,1024]{1,0:T(8,128)(2,1)S(1)} %slice.56), channel_id=1, source_target_pairs={{0,224},{32,0},{64,32},{96,64},{128,96},{160,128},{192,160},{224,1... | collective-permute-start | bytes 786440 | tf_op jit(solution)/shard_map/ppermute | solution.py:20
  100.2 4.3 %collective-permute-done.10.refs_8_.refs_5_ = bf16[128,1024]{1,0:T(8,128)(2,1)S(1)} collective-permute-done((bf16[128,1024]{1,0:T(8,128)(2,1)S(1)}, bf16[128,1024]{1,0:T(8,128)(2,1)S(1)}, u32[]{:S(2)}, u32[]{:S(2)}) %collective-permute-start.10) | collective-permute-done | bytes 262176 | tf_op jit(solution)/shard_map/ppermute | solution.py:20
  104.9 2.3 %collective-permute-start.22 = (bf16[192,1024]{1,0:T(8,128)(2,1)S(1)}, bf16[192,1024]{1,0:T(8,128)(2,1)S(1)}, u32[]{:S(2)}, u32[]{:S(2)}) collective-permute-start(bf16[192,1024]{1,0:T(8,128)(2,1)S(1)} %constant_dynamic-update-slice_fusion.5.refs_4_.a_ref), channel_id=1, source_target_pairs={{0,16},{8,24},{16,0},{24,8},{1,17},{9,25},{17,1},{25,9},{2,18},{10... | collective-permute-start | bytes 1179656 | tf_op jit(solution)/shard_map/ppermute | solution.py:20
  107.2 1.3 collective-permute-start.23
  108.5 4.6 %up.3.refs_6_ = f32[1024,1024]{1,0:T(8,128)S(1)} custom-call(bf16[512,2048]{1,0:T(8,128)(2,1)S(1)} %place.5.refs_0_.refs_1_.refs_2_.refs_3_.refs_4_, bf16[512,2048]{1,0:T(8,128)(2,1)S(1)} %place.5.refs_0_.refs_1_.refs_2_.refs_3_.refs_4_, bf16[512,2048]{1,0:T(8,128)(2,1)S(1)} %place.5.refs_0_.refs_1_.refs_2_.refs_3_.refs_4_, ...), custom_call_target="tpu_custom_call" | custom-call | flops 2684354560 | bytes 6291456 | tf_op jit(solution)/shard_map/up/pallas_call | solution.py:106
  113.1 2.8 %up.4.refs_6_ = f32[1024,1024]{1,0:T(8,128)S(1)} custom-call(bf16[512,2048]{1,0:T(8,128)(2,1)S(1)} %place.5.refs_0_.refs_1_.refs_2_.refs_3_.refs_4_, bf16[512,2048]{1,0:T(8,128)(2,1)S(1)} %place.5.refs_0_.refs_1_.refs_2_.refs_3_.refs_4_, bf16[512,2048]{1,0:T(8,128)(2,1)S(1)} %collective-permute-done.27.refs_5_.refs_6_.refs_7_.refs_8_.refs_9_.refs_2_.refs_3_, ...), custom_call_target="tpu_custom_call" | custom-call | flops 1073741824 | bytes 6291456 | tf_op jit(solution)/shard_map/up/pallas_call | solution.py:106
  115.9 2.1 %up.5.h_ref = bf16[1024,1024]{1,0:T(8,128)(2,1)S(1)} custom-call(bf16[512,2048]{1,0:T(8,128)(2,1)S(1)} %place.5.refs_0_.refs_1_.refs_2_.refs_3_.refs_4_, bf16[512,2048]{1,0:T(8,128)(2,1)S(1)} %place.5.refs_0_.refs_1_.refs_2_.refs_3_.refs_4_, bf16[512,2048]{1,0:T(8,128)(2,1)S(1)} %collective-permute-done.27.refs_5_.refs_6_.refs_7_.refs_8_.refs_9_.refs_2_.refs_3_, ...), custom_call_target="tpu_custom_call" | custom-call | flops 536870912 | bytes 6291456 | tf_op jit(solution)/shard_map/up/pallas_call | solution.py:106
  118.0 7.7 %collective-permute-done.17.refs_3_.d_ref = bf16[320,1024]{1,0:T(8,128)(2,1)S(1)} collective-permute-done((bf16[320,1024]{1,0:T(8,128)(2,1)S(1)}, bf16[320,1024]{1,0:T(8,128)(2,1)S(1)}, u32[]{:S(2)}, u32[]{:S(2)}) %collective-permute-start.17) | collective-permute-done | bytes 655392 | tf_op jit(solution)/shard_map/ppermute | solution.py:20
  125.7 1.6 down.3
  127.4 12.7 %collective-permute-done.23.refs_7_.d_ref = bf16[192,1024]{1,0:T(8,128)(2,1)S(1)} collective-permute-done((bf16[192,1024]{1,0:T(8,128)(2,1)S(1)}, bf16[192,1024]{1,0:T(8,128)(2,1)S(1)}, u32[]{:S(2)}, u32[]{:S(2)}) %collective-permute-start.23) | collective-permute-done | bytes 393248 | tf_op jit(solution)/shard_map/ppermute | solution.py:20
  140.1 2.3 %down.5 = (bf16[512,768]{1,0:T(8,128)(2,1)S(1)}, bf16[512,768]{1,0:T(8,128)(2,1)S(1)}) custom-call(bf16[1024,1024]{1,0:T(8,128)(2,1)S(1)} %up.5.h_ref, bf16[192,1024]{1,0:T(8,128)(2,1)S(1)} %constant_dynamic-update-slice_fusion.5.refs_4_.a_ref, bf16[192,1024]{1,0:T(8,128)(2,1)S(1)} %collective-permute-done.21.refs_5_.b_ref, ...), custom_call_target="tpu_custom_call" | custom-call | flops 1610612736 | bytes 6291456 | tf_op jit(solution)/shard_map/down/pallas_call | solution.py:134
  142.8 2.4 %down.4 = (bf16[512,768]{1,0:T(8,128)(2,1)S(1)}, bf16[512,768]{1,0:T(8,128)(2,1)S(1)}) custom-call(bf16[1024,1024]{1,0:T(8,128)(2,1)S(1)} %up.5.h_ref, bf16[320,1024]{1,0:T(8,128)(2,1)S(1)} %constant_dynamic-update-slice_fusion.refs_0_.a_ref, bf16[320,1024]{1,0:T(8,128)(2,1)S(1)} %collective-permute-done.15.refs_1_.b_ref, ...), custom_call_target="tpu_custom_call" | custom-call | flops 1610612736 | bytes 6291456 | tf_op jit(solution)/shard_map/down/pallas_call | solution.py:134
  146.0 2.1 %collective-permute-start.30 = (bf16[128,512]{1,0:T(8,128)(2,1)S(1)}, bf16[128,512]{1,0:T(8,128)(2,1)S(1)}, u32[]{:S(2)}, u32[]{:S(2)}) collective-permute-start(bf16[128,512]{1,0:T(8,128)(2,1)S(1)} %get-tuple-element.26), channel_id=1, source_target_pairs={{0,4},{2,6},{4,0},{6,2},{1,5},{3,7},{5,1},{7,3},{8,12},{10,14},{12... | collective-permute-start | bytes 393224 | tf_op jit(solution)/shard_map/ppermute | solution.py:20
  148.1 1.3 collective-permute-start.31
  150.5 2.2 %collective-permute-start.38 = (bf16[128,768]{1,0:T(8,128)(2,1)S(1)}, bf16[128,768]{1,0:T(8,128)(2,1)S(1)}, u32[]{:S(2)}, u32[]{:S(2)}) collective-permute-start(bf16[128,768]{1,0:T(8,128)(2,1)S(1)} %get-tuple-element.18), channel_id=1, source_target_pairs={{0,4},{2,6},{4,0},{6,2},{1,5},{3,7},{5,1},{7,3},{8,12},{10,14},{12... | collective-permute-start | bytes 589832 | tf_op jit(solution)/shard_map/ppermute | solution.py:20
  152.9 3.4 %collective-permute-done.29.refs_1_ = bf16[128,512]{1,0:T(8,128)(2,1)S(1)} collective-permute-done((bf16[128,512]{1,0:T(8,128)(2,1)S(1)}, bf16[128,512]{1,0:T(8,128)(2,1)S(1)}, u32[]{:S(2)}, u32[]{:S(2)}) %collective-permute-start.29) | collective-permute-done | bytes 131104 | tf_op jit(solution)/shard_map/ppermute | solution.py:20
  156.3 2.0 %collective-permute-start.33 = (bf16[128,768]{1,0:T(8,128)(2,1)S(1)}, bf16[128,768]{1,0:T(8,128)(2,1)S(1)}, u32[]{:S(2)}, u32[]{:S(2)}) collective-permute-start(bf16[128,768]{1,0:T(8,128)(2,1)S(1)} %get-tuple-element.23), channel_id=1, source_target_pairs={{0,2},{2,4},{4,6},{6,0},{1,3},{3,5},{5,7},{7,1},{8,10},{10,12},{12... | collective-permute-start | bytes 589832 | tf_op jit(solution)/shard_map/ppermute | solution.py:20
  158.3 1.3 collective-permute-start.34
  159.7 5.1 %collective-permute-done.37.refs_9_ = bf16[128,768]{1,0:T(8,128)(2,1)S(1)} collective-permute-done((bf16[128,768]{1,0:T(8,128)(2,1)S(1)}, bf16[128,768]{1,0:T(8,128)(2,1)S(1)}, u32[]{:S(2)}, u32[]{:S(2)}) %collective-permute-start.37) | collective-permute-done | bytes 196640 | tf_op jit(solution)/shard_map/ppermute | solution.py:20
  164.7 2.9 %turn.1 = bf16[1024,2048]{1,0:T(8,128)(2,1)} custom-call(bf16[320,1024]{1,0:T(8,128)(2,1)S(1)} %constant_dynamic-update-slice_fusion.refs_0_.a_ref, bf16[320,1024]{1,0:T(8,128)(2,1)S(1)} %collective-permute-done.15.refs_1_.b_ref, bf16[320,1024]{1,0:T(8,128)(2,1)S(1)} %collective-permute-done.16.refs_2_.c_ref, ...), custom_call_target="tpu_custom_call" | custom-call | flops 2000000000 | bytes 8388608 | tf_op jit(solution)/shard_map/turn/pallas_call | solution.py:176
  167.7 2.1 %place.4 = bf16[2048,1024]{1,0:T(8,128)(2,1)} custom-call(bf16[256,1024]{1,0:T(8,128)(2,1)S(1)} %collective-permute-done.4.refs_0_.refs_10_, bf16[256,1024]{1,0:T(8,128)(2,1)S(1)} %collective-permute-done.3.refs_1_.refs_11_, bf16[256,1024]{1,0:T(8,128)(2,1)S(1)} %place.3.refs_2_.refs_12_, bf16[256,1024]{1,0:T(8,128)(2,1)S(1)} %collective-permute-done.5.refs_3_.refs_13_, ...), custom_call_target="tpu_custom_call" | custom-call | tf_op jit(solution)/shard_map/place/pallas_call | solution.py:71
  169.8 2.5 %collective-permute-done.33.refs_5_ = bf16[128,768]{1,0:T(8,128)(2,1)S(1)} collective-permute-done((bf16[128,768]{1,0:T(8,128)(2,1)S(1)}, bf16[128,768]{1,0:T(8,128)(2,1)S(1)}, u32[]{:S(2)}, u32[]{:S(2)}) %collective-permute-start.33) | collective-permute-done | bytes 196640 | tf_op jit(solution)/shard_map/ppermute | solution.py:20
  173.0 1.2 total.1
  (65 shorter events, 9.2 us)
Async XLA Ops:
  0.6 1.0 copy-start
  1.9 25.3 %collective-permute-start.24 = (bf16[128,2048]{1,0:T(8,128)(2,1)S(1)}, bf16[128,2048]{1,0:T(8,128)(2,1)S(1)}, u32[]{:S(2)}, u32[]{:S(2)}) collective-permute-start(bf16[128,2048]{1,0:T(8,128)(2,1)S(1)} %norm.1.refs_0_), channel_id=1, source_target_pairs={{0,6},{2,0},{4,2},{6,4},{1,7},{3,1},{5,3},{7,5},{8,14},{10,8},{12,... | collective-permute-start | bytes 1572872 | tf_op jit(solution)/shard_map/ppermute | solution.py:20
  4.7 22.5 %collective-permute-start.25 = (bf16[128,2048]{1,0:T(8,128)(2,1)S(1)}, bf16[128,2048]{1,0:T(8,128)(2,1)S(1)}, u32[]{:S(2)}, u32[]{:S(2)}) collective-permute-start(bf16[128,2048]{1,0:T(8,128)(2,1)S(1)} %norm.1.refs_0_), channel_id=1, source_target_pairs={{0,4},{2,6},{4,0},{6,2},{1,5},{3,7},{5,1},{7,3},{8,12},{10,14},{12... | collective-permute-start | bytes 1572872 | tf_op jit(solution)/shard_map/ppermute | solution.py:20
  5.5 25.3 %collective-permute-start.26 = (bf16[128,2048]{1,0:T(8,128)(2,1)S(1)}, bf16[128,2048]{1,0:T(8,128)(2,1)S(1)}, u32[]{:S(2)}, u32[]{:S(2)}) collective-permute-start(bf16[128,2048]{1,0:T(8,128)(2,1)S(1)} %norm.1.refs_0_), channel_id=1, source_target_pairs={{0,2},{2,4},{4,6},{6,0},{1,3},{3,5},{5,7},{7,1},{8,10},{10,12},{12... | collective-permute-start | bytes 1572872 | tf_op jit(solution)/shard_map/ppermute | solution.py:20
  7.4 6.4 %collective-permute-start = (bf16[64,1024]{1,0:T(8,128)(2,1)S(1)}, bf16[64,1024]{1,0:T(8,128)(2,1)S(1)}, u32[]{:S(2)}, u32[]{:S(2)}) collective-permute-start(bf16[64,1024]{1,0:T(8,128)(2,1)S(1)} %multiply_convert_fusion.refs_0_), channel_id=1, source_target_pairs={{0,24},{8,0},{16,8},{24,16},{1,25},{9,1},{17,9},{25,17},{2,26},{10... | collective-permute-start | bytes 393224 | tf_op jit(solution)/shard_map/ppermute | solution.py:20
  8.0 7.8 %collective-permute-start.1 = (bf16[64,1024]{1,0:T(8,128)(2,1)S(1)}, bf16[64,1024]{1,0:T(8,128)(2,1)S(1)}, u32[]{:S(2)}, u32[]{:S(2)}) collective-permute-start(bf16[64,1024]{1,0:T(8,128)(2,1)S(1)} %multiply_convert_fusion.refs_0_), channel_id=1, source_target_pairs={{0,16},{8,24},{16,0},{24,8},{1,17},{9,25},{17,1},{25,9},{2,18},{10... | collective-permute-start | bytes 393224 | tf_op jit(solution)/shard_map/ppermute | solution.py:20
  13.9 5.0 %collective-permute-start.2 = (bf16[64,1024]{1,0:T(8,128)(2,1)S(1)}, bf16[64,1024]{1,0:T(8,128)(2,1)S(1)}, u32[]{:S(2)}, u32[]{:S(2)}) collective-permute-start(bf16[64,1024]{1,0:T(8,128)(2,1)S(1)} %multiply_convert_fusion.refs_0_), channel_id=1, source_target_pairs={{0,8},{8,16},{16,24},{24,0},{1,9},{9,17},{17,25},{25,1},{2,10},{10... | collective-permute-start | bytes 393224 | tf_op jit(solution)/shard_map/ppermute | solution.py:20
  19.6 17.5 %copy-start.1 = (f32[64,1024]{1,0:T(8,128)S(1)}, f32[64,1024]{1,0:T(8,128)}, u32[]{:S(2)}) copy-start(f32[64,1024]{1,0:T(8,128)} %param.7) | copy-start | bytes 786436
  19.6 17.5 %collective-permute-start.3 = (bf16[256,1024]{1,0:T(8,128)(2,1)S(1)}, bf16[256,1024]{1,0:T(8,128)(2,1)S(1)}, u32[]{:S(2)}, u32[]{:S(2)}) collective-permute-start(bf16[256,1024]{1,0:T(8,128)(2,1)S(1)} %place.3.refs_2_.refs_12_), channel_id=1, source_target_pairs={{0,32},{32,64},{64,96},{96,128},{128,160},{160,192},{192,224},{224... | collective-permute-start | bytes 1572872 | tf_op jit(solution)/shard_map/ppermute | solution.py:20
  31.0 76.2 %collective-permute-start.27 = (bf16[512,2048]{1,0:T(8,128)(2,1)S(1)}, bf16[512,2048]{1,0:T(8,128)(2,1)S(1)}, u32[]{:S(2)}, u32[]{:S(2)}) collective-permute-start(bf16[512,2048]{1,0:T(8,128)(2,1)S(1)} %place.5.refs_0_.refs_1_.refs_2_.refs_3_.refs_4_), channel_id=1, source_target_pairs={{0,1},{1,0},{2,3},{3,2},{4,5},{5,4},{6,7},{7,6},{8,9},{9,8},{10,11... | collective-permute-start | bytes 6291464 | tf_op jit(solution)/shard_map/ppermute | solution.py:20
  31.1 23.4 %collective-permute-start.5 = (bf16[256,1024]{1,0:T(8,128)(2,1)S(1)}, bf16[256,1024]{1,0:T(8,128)(2,1)S(1)}, u32[]{:S(2)}, u32[]{:S(2)}) collective-permute-start(bf16[256,1024]{1,0:T(8,128)(2,1)S(1)} %place.3.refs_2_.refs_12_), channel_id=1, source_target_pairs={{0,224},{32,0},{64,32},{96,64},{128,96},{160,128},{192,160},{224,1... | collective-permute-start | bytes 1572872 | tf_op jit(solution)/shard_map/ppermute | solution.py:20
  37.1 24.1 %collective-permute-start.4 = (bf16[256,1024]{1,0:T(8,128)(2,1)S(1)}, bf16[256,1024]{1,0:T(8,128)(2,1)S(1)}, u32[]{:S(2)}, u32[]{:S(2)}) collective-permute-start(bf16[256,1024]{1,0:T(8,128)(2,1)S(1)} %collective-permute-done.3.refs_1_.refs_11_), channel_id=1, source_target_pairs={{0,32},{32,64},{64,96},{96,128},{128,160},{160,192},{192,224},{224... | collective-permute-start | bytes 1572872 | tf_op jit(solution)/shard_map/ppermute | solution.py:20
  37.1 14.5 %collective-permute-start.11 = (bf16[64,1024]{1,0:T(8,128)(2,1)S(1)}, bf16[64,1024]{1,0:T(8,128)(2,1)S(1)}, u32[]{:S(2)}, u32[]{:S(2)}) collective-permute-start(bf16[64,1024]{1,0:T(8,128)(2,1)S(1)} %get-tuple-element.16), channel_id=1, source_target_pairs={{0,224},{32,0},{64,32},{96,64},{128,96},{160,128},{192,160},{224,1... | collective-permute-start | bytes 393224 | tf_op jit(solution)/shard_map/ppermute | solution.py:20
  40.4 15.2 %collective-permute-start.12 = (bf16[64,1024]{1,0:T(8,128)(2,1)S(1)}, bf16[64,1024]{1,0:T(8,128)(2,1)S(1)}, u32[]{:S(2)}, u32[]{:S(2)}) collective-permute-start(bf16[64,1024]{1,0:T(8,128)(2,1)S(1)} %get-tuple-element.16), channel_id=1, source_target_pairs={{0,32},{32,64},{64,96},{96,128},{128,160},{160,192},{192,224},{224... | collective-permute-start | bytes 393224 | tf_op jit(solution)/shard_map/ppermute | solution.py:20
  51.6 9.5 %collective-permute-start.13 = (bf16[64,1024]{1,0:T(8,128)(2,1)S(1)}, bf16[64,1024]{1,0:T(8,128)(2,1)S(1)}, u32[]{:S(2)}, u32[]{:S(2)}) collective-permute-start(bf16[64,1024]{1,0:T(8,128)(2,1)S(1)} %get-tuple-element.16), channel_id=1, source_target_pairs={{0,192},{32,224},{64,0},{96,32},{128,64},{160,96},{192,128},{224,1... | collective-permute-start | bytes 393224 | tf_op jit(solution)/shard_map/ppermute | solution.py:20
  54.6 18.0 %collective-permute-start.6 = (bf16[256,1024]{1,0:T(8,128)(2,1)S(1)}, bf16[256,1024]{1,0:T(8,128)(2,1)S(1)}, u32[]{:S(2)}, u32[]{:S(2)}) collective-permute-start(bf16[256,1024]{1,0:T(8,128)(2,1)S(1)} %collective-permute-done.5.refs_3_.refs_13_), channel_id=1, source_target_pairs={{0,224},{32,0},{64,32},{96,64},{128,96},{160,128},{192,160},{224,1... | collective-permute-start | bytes 1572872 | tf_op jit(solution)/shard_map/ppermute | solution.py:20
  55.6 8.8 %collective-permute-start.14 = (bf16[64,1024]{1,0:T(8,128)(2,1)S(1)}, bf16[64,1024]{1,0:T(8,128)(2,1)S(1)}, u32[]{:S(2)}, u32[]{:S(2)}) collective-permute-start(bf16[64,1024]{1,0:T(8,128)(2,1)S(1)} %get-tuple-element.16), channel_id=1, source_target_pairs={{0,64},{32,96},{64,128},{96,160},{128,192},{160,224},{192,0},{224,... | collective-permute-start | bytes 393224 | tf_op jit(solution)/shard_map/ppermute | solution.py:20
  61.1 28.0 %collective-permute-start.7 = (bf16[256,1024]{1,0:T(8,128)(2,1)S(1)}, bf16[256,1024]{1,0:T(8,128)(2,1)S(1)}, u32[]{:S(2)}, u32[]{:S(2)}) collective-permute-start(bf16[256,1024]{1,0:T(8,128)(2,1)S(1)} %collective-permute-done.4.refs_0_.refs_10_), channel_id=1, source_target_pairs={{0,32},{32,64},{64,96},{96,128},{128,160},{160,192},{192,224},{224... | collective-permute-start | bytes 1572872 | tf_op jit(solution)/shard_map/ppermute | solution.py:20
  64.4 32.5 %collective-permute-start.15 = (bf16[320,1024]{1,0:T(8,128)(2,1)S(1)}, bf16[320,1024]{1,0:T(8,128)(2,1)S(1)}, u32[]{:S(2)}, u32[]{:S(2)}) collective-permute-start(bf16[320,1024]{1,0:T(8,128)(2,1)S(1)} %constant_dynamic-update-slice_fusion.refs_0_.a_ref), channel_id=1, source_target_pairs={{0,24},{8,0},{16,8},{24,16},{1,25},{9,1},{17,9},{25,17},{2,26},{10... | collective-permute-start | bytes 1966088 | tf_op jit(solution)/shard_map/ppermute | solution.py:20
  72.6 19.8 %collective-permute-start.8 = (bf16[256,1024]{1,0:T(8,128)(2,1)S(1)}, bf16[256,1024]{1,0:T(8,128)(2,1)S(1)}, u32[]{:S(2)}, u32[]{:S(2)}) collective-permute-start(bf16[256,1024]{1,0:T(8,128)(2,1)S(1)} %collective-permute-done.6.refs_4_.refs_14_), channel_id=1, source_target_pairs={{0,224},{32,0},{64,32},{96,64},{128,96},{160,128},{192,160},{224,1... | collective-permute-start | bytes 1572872 | tf_op jit(solution)/shard_map/ppermute | solution.py:20
  74.8 14.3 %collective-permute-start.18 = (bf16[64,1024]{1,0:T(8,128)(2,1)S(1)}, bf16[64,1024]{1,0:T(8,128)(2,1)S(1)}, u32[]{:S(2)}, u32[]{:S(2)}) collective-permute-start(bf16[64,1024]{1,0:T(8,128)(2,1)S(1)} %collective-permute-done.13), channel_id=1, source_target_pairs={{0,224},{32,0},{64,32},{96,64},{128,96},{160,128},{192,160},{224,1... | collective-permute-start | bytes 393224 | tf_op jit(solution)/shard_map/ppermute | solution.py:20
  89.1 6.2 %collective-permute-start.19 = (bf16[64,1024]{1,0:T(8,128)(2,1)S(1)}, bf16[64,1024]{1,0:T(8,128)(2,1)S(1)}, u32[]{:S(2)}, u32[]{:S(2)}) collective-permute-start(bf16[64,1024]{1,0:T(8,128)(2,1)S(1)} %collective-permute-done.14), channel_id=1, source_target_pairs={{0,32},{32,64},{64,96},{96,128},{128,160},{160,192},{192,224},{224... | collective-permute-start | bytes 393224 | tf_op jit(solution)/shard_map/ppermute | solution.py:20
  89.1 7.8 %collective-permute-start.20 = (bf16[64,1024]{1,0:T(8,128)(2,1)S(1)}, bf16[64,1024]{1,0:T(8,128)(2,1)S(1)}, u32[]{:S(2)}, u32[]{:S(2)}) collective-permute-start(bf16[64,1024]{1,0:T(8,128)(2,1)S(1)} %collective-permute-done.18), channel_id=1, source_target_pairs={{0,224},{32,0},{64,32},{96,64},{128,96},{160,128},{192,160},{224,1... | collective-permute-start | bytes 393224 | tf_op jit(solution)/shard_map/ppermute | solution.py:20
  92.4 25.6 %collective-permute-start.16 = (bf16[320,1024]{1,0:T(8,128)(2,1)S(1)}, bf16[320,1024]{1,0:T(8,128)(2,1)S(1)}, u32[]{:S(2)}, u32[]{:S(2)}) collective-permute-start(bf16[320,1024]{1,0:T(8,128)(2,1)S(1)} %constant_dynamic-update-slice_fusion.refs_0_.a_ref), channel_id=1, source_target_pairs={{0,16},{8,24},{16,0},{24,8},{1,17},{9,25},{17,1},{25,9},{2,18},{10... | collective-permute-start | bytes 1966088 | tf_op jit(solution)/shard_map/ppermute | solution.py:20
  95.3 30.5 %collective-permute-start.17 = (bf16[320,1024]{1,0:T(8,128)(2,1)S(1)}, bf16[320,1024]{1,0:T(8,128)(2,1)S(1)}, u32[]{:S(2)}, u32[]{:S(2)}) collective-permute-start(bf16[320,1024]{1,0:T(8,128)(2,1)S(1)} %constant_dynamic-update-slice_fusion.refs_0_.a_ref), channel_id=1, source_target_pairs={{0,8},{8,16},{16,24},{24,0},{1,9},{9,17},{17,25},{25,1},{2,10},{10... | collective-permute-start | bytes 1966088 | tf_op jit(solution)/shard_map/ppermute | solution.py:20
  96.9 7.6 %collective-permute-start.10 = (bf16[128,1024]{1,0:T(8,128)(2,1)S(1)}, bf16[128,1024]{1,0:T(8,128)(2,1)S(1)}, u32[]{:S(2)}, u32[]{:S(2)}) collective-permute-start(bf16[128,1024]{1,0:T(8,128)(2,1)S(1)} %slice.57), channel_id=1, source_target_pairs={{0,32},{32,64},{64,96},{96,128},{128,160},{160,192},{192,224},{224... | collective-permute-start | bytes 786440 | tf_op jit(solution)/shard_map/ppermute | solution.py:20
  96.9 8.0 %collective-permute-start.9 = (bf16[128,1024]{1,0:T(8,128)(2,1)S(1)}, bf16[128,1024]{1,0:T(8,128)(2,1)S(1)}, u32[]{:S(2)}, u32[]{:S(2)}) collective-permute-start(bf16[128,1024]{1,0:T(8,128)(2,1)S(1)} %slice.56), channel_id=1, source_target_pairs={{0,224},{32,0},{64,32},{96,64},{128,96},{160,128},{192,160},{224,1... | collective-permute-start | bytes 786440 | tf_op jit(solution)/shard_map/ppermute | solution.py:20
  104.4 23.0 %collective-permute-start.21 = (bf16[192,1024]{1,0:T(8,128)(2,1)S(1)}, bf16[192,1024]{1,0:T(8,128)(2,1)S(1)}, u32[]{:S(2)}, u32[]{:S(2)}) collective-permute-start(bf16[192,1024]{1,0:T(8,128)(2,1)S(1)} %constant_dynamic-update-slice_fusion.5.refs_4_.a_ref), channel_id=1, source_target_pairs={{0,24},{8,0},{16,8},{24,16},{1,25},{9,1},{17,9},{25,17},{2,26},{10... | collective-permute-start | bytes 1179656 | tf_op jit(solution)/shard_map/ppermute | solution.py:20
  104.9 22.5 %collective-permute-start.22 = (bf16[192,1024]{1,0:T(8,128)(2,1)S(1)}, bf16[192,1024]{1,0:T(8,128)(2,1)S(1)}, u32[]{:S(2)}, u32[]{:S(2)}) collective-permute-start(bf16[192,1024]{1,0:T(8,128)(2,1)S(1)} %constant_dynamic-update-slice_fusion.5.refs_4_.a_ref), channel_id=1, source_target_pairs={{0,16},{8,24},{16,0},{24,8},{1,17},{9,25},{17,1},{25,9},{2,18},{10... | collective-permute-start | bytes 1179656 | tf_op jit(solution)/shard_map/ppermute | solution.py:20
  107.2 32.9 %collective-permute-start.23 = (bf16[192,1024]{1,0:T(8,128)(2,1)S(1)}, bf16[192,1024]{1,0:T(8,128)(2,1)S(1)}, u32[]{:S(2)}, u32[]{:S(2)}) collective-permute-start(bf16[192,1024]{1,0:T(8,128)(2,1)S(1)} %constant_dynamic-update-slice_fusion.5.refs_4_.a_ref), channel_id=1, source_target_pairs={{0,8},{8,16},{16,24},{24,0},{1,9},{9,17},{17,25},{25,1},{2,10},{10... | collective-permute-start | bytes 1179656 | tf_op jit(solution)/shard_map/ppermute | solution.py:20
  127.3 18.4 %collective-permute-start.28 = (bf16[512,512]{1,0:T(8,128)(2,1)S(1)}, bf16[512,512]{1,0:T(8,128)(2,1)S(1)}, u32[]{:S(2)}, u32[]{:S(2)}) collective-permute-start(bf16[512,512]{1,0:T(8,128)(2,1)S(1)} %get-tuple-element.10), channel_id=1, source_target_pairs={{0,1},{1,0},{2,3},{3,2},{4,5},{5,4},{6,7},{7,6},{8,9},{9,8},{10,11... | collective-permute-start | bytes 1572872 | tf_op jit(solution)/shard_map/ppermute | solution.py:20
  142.5 7.0 %collective-permute-start.36 = (bf16[512,768]{1,0:T(8,128)(2,1)S(1)}, bf16[512,768]{1,0:T(8,128)(2,1)S(1)}, u32[]{:S(2)}, u32[]{:S(2)}) collective-permute-start(bf16[512,768]{1,0:T(8,128)(2,1)S(1)} %get-tuple-element.14), channel_id=1, source_target_pairs={{0,1},{1,0},{2,3},{3,2},{4,5},{5,4},{6,7},{7,6},{8,9},{9,8},{10,11... | collective-permute-start | bytes 2359304 | tf_op jit(solution)/shard_map/ppermute | solution.py:20
  145.2 5.3 %collective-permute-start.32 = (bf16[512,768]{1,0:T(8,128)(2,1)S(1)}, bf16[512,768]{1,0:T(8,128)(2,1)S(1)}, u32[]{:S(2)}, u32[]{:S(2)}) collective-permute-start(bf16[512,768]{1,0:T(8,128)(2,1)S(1)} %get-tuple-element.12), channel_id=1, source_target_pairs={{0,1},{1,0},{2,3},{3,2},{4,5},{5,4},{6,7},{7,6},{8,9},{9,8},{10,11... | collective-permute-start | bytes 2359304 | tf_op jit(solution)/shard_map/ppermute | solution.py:20
  145.9 10.4 %collective-permute-start.29 = (bf16[128,512]{1,0:T(8,128)(2,1)S(1)}, bf16[128,512]{1,0:T(8,128)(2,1)S(1)}, u32[]{:S(2)}, u32[]{:S(2)}) collective-permute-start(bf16[128,512]{1,0:T(8,128)(2,1)S(1)} %get-tuple-element.27), channel_id=1, source_target_pairs={{0,2},{2,4},{4,6},{6,0},{1,3},{3,5},{5,7},{7,1},{8,10},{10,12},{12... | collective-permute-start | bytes 393224 | tf_op jit(solution)/shard_map/ppermute | solution.py:20
  146.0 10.3 %collective-permute-start.30 = (bf16[128,512]{1,0:T(8,128)(2,1)S(1)}, bf16[128,512]{1,0:T(8,128)(2,1)S(1)}, u32[]{:S(2)}, u32[]{:S(2)}) collective-permute-start(bf16[128,512]{1,0:T(8,128)(2,1)S(1)} %get-tuple-element.26), channel_id=1, source_target_pairs={{0,4},{2,6},{4,0},{6,2},{1,5},{3,7},{5,1},{7,3},{8,12},{10,14},{12... | collective-permute-start | bytes 393224 | tf_op jit(solution)/shard_map/ppermute | solution.py:20
  148.1 10.2 %collective-permute-start.31 = (bf16[128,512]{1,0:T(8,128)(2,1)S(1)}, bf16[128,512]{1,0:T(8,128)(2,1)S(1)}, u32[]{:S(2)}, u32[]{:S(2)}) collective-permute-start(bf16[128,512]{1,0:T(8,128)(2,1)S(1)} %get-tuple-element.25), channel_id=1, source_target_pairs={{0,6},{2,0},{4,2},{6,4},{1,7},{3,1},{5,3},{7,5},{8,14},{10,8},{12,... | collective-permute-start | bytes 393224 | tf_op jit(solution)/shard_map/ppermute | solution.py:20
  149.7 15.0 %collective-permute-start.37 = (bf16[128,768]{1,0:T(8,128)(2,1)S(1)}, bf16[128,768]{1,0:T(8,128)(2,1)S(1)}, u32[]{:S(2)}, u32[]{:S(2)}) collective-permute-start(bf16[128,768]{1,0:T(8,128)(2,1)S(1)} %get-tuple-element.19), channel_id=1, source_target_pairs={{0,2},{2,4},{4,6},{6,0},{1,3},{3,5},{5,7},{7,1},{8,10},{10,12},{12... | collective-permute-start | bytes 589832 | tf_op jit(solution)/shard_map/ppermute | solution.py:20
  150.5 19.3 %collective-permute-start.38 = (bf16[128,768]{1,0:T(8,128)(2,1)S(1)}, bf16[128,768]{1,0:T(8,128)(2,1)S(1)}, u32[]{:S(2)}, u32[]{:S(2)}) collective-permute-start(bf16[128,768]{1,0:T(8,128)(2,1)S(1)} %get-tuple-element.18), channel_id=1, source_target_pairs={{0,4},{2,6},{4,0},{6,2},{1,5},{3,7},{5,1},{7,3},{8,12},{10,14},{12... | collective-permute-start | bytes 589832 | tf_op jit(solution)/shard_map/ppermute | solution.py:20
  156.3 13.5 %collective-permute-start.39 = (bf16[128,768]{1,0:T(8,128)(2,1)S(1)}, bf16[128,768]{1,0:T(8,128)(2,1)S(1)}, u32[]{:S(2)}, u32[]{:S(2)}) collective-permute-start(bf16[128,768]{1,0:T(8,128)(2,1)S(1)} %get-tuple-element.17), channel_id=1, source_target_pairs={{0,6},{2,0},{4,2},{6,4},{1,7},{3,1},{5,3},{7,5},{8,14},{10,8},{12,... | collective-permute-start | bytes 589832 | tf_op jit(solution)/shard_map/ppermute | solution.py:20
  156.3 16.0 %collective-permute-start.33 = (bf16[128,768]{1,0:T(8,128)(2,1)S(1)}, bf16[128,768]{1,0:T(8,128)(2,1)S(1)}, u32[]{:S(2)}, u32[]{:S(2)}) collective-permute-start(bf16[128,768]{1,0:T(8,128)(2,1)S(1)} %get-tuple-element.23), channel_id=1, source_target_pairs={{0,2},{2,4},{4,6},{6,0},{1,3},{3,5},{5,7},{7,1},{8,10},{10,12},{12... | collective-permute-start | bytes 589832 | tf_op jit(solution)/shard_map/ppermute | solution.py:20
  158.3 14.0 %collective-permute-start.34 = (bf16[128,768]{1,0:T(8,128)(2,1)S(1)}, bf16[128,768]{1,0:T(8,128)(2,1)S(1)}, u32[]{:S(2)}, u32[]{:S(2)}) collective-permute-start(bf16[128,768]{1,0:T(8,128)(2,1)S(1)} %get-tuple-element.22), channel_id=1, source_target_pairs={{0,4},{2,6},{4,0},{6,2},{1,5},{3,7},{5,1},{7,3},{8,12},{10,14},{12... | collective-permute-start | bytes 589832 | tf_op jit(solution)/shard_map/ppermute | solution.py:20
  164.7 8.3 %collective-permute-start.35 = (bf16[128,768]{1,0:T(8,128)(2,1)S(1)}, bf16[128,768]{1,0:T(8,128)(2,1)S(1)}, u32[]{:S(2)}, u32[]{:S(2)}) collective-permute-start(bf16[128,768]{1,0:T(8,128)(2,1)S(1)} %get-tuple-element.21), channel_id=1, source_target_pairs={{0,6},{2,0},{4,2},{6,4},{1,7},{3,1},{5,3},{7,5},{8,14},{10,8},{12,... | collective-permute-start | bytes 589832 | tf_op jit(solution)/shard_map/ppermute | solution.py:20

commit v2 on v1

--- a/solution.py
+++ b/solution.py
@@ -79,65 +79,66 @@
     )(*parts)
 
 
-def up_kernel(n, more, last, *refs):
-    own, oth, parts, o_ref = refs[:n], refs[n : 2 * n], refs[2 * n : 3 * n], refs[-1]
-    half = own[0].shape[0]
-    rhs = jnp.concatenate([p[...] for p in parts], axis=0)
-    for c, group in enumerate((own, oth)):
-        lhs = jnp.concatenate([t[...] for t in group], axis=1)
-        dot = jnp.dot(lhs, rhs, preferred_element_type=jnp.float32)
-        if more:
-            dot = dot + refs[3 * n][c * half : (c + 1) * half, :]
-        if last:
-            dot = jnp.square(jnp.maximum(dot, 0.0))
-        o_ref[c * half : (c + 1) * half, :] = dot.astype(o_ref.dtype)
+def up_kernel(places, more, last, *refs):
+    n, o_ref = len(places), refs[-1]
+    parts = refs[2 : 2 + n]
+    half, tile = refs[0].shape[0], 256
+
+    @pl.loop(0, o_ref.shape[1] // tile)
+    def _(j):
+        cols = pl.ds(pl.multiple_of(j * tile, tile), tile)
+        rhs = jnp.concatenate([p[:, cols] for p in parts], axis=0)
+        for c in range(2):
+            rows = slice(c * half, (c + 1) * half)
+            lhs = [refs[c][:, at : at + p.shape[0]] for p, at in zip(parts, places)]
+            lhs = jnp.concatenate(lhs, axis=1)
+            dot = jnp.dot(lhs, rhs, preferred_element_type=jnp.float32)
+            if more:
+                dot = dot + refs[2 + n][rows, cols]
+            if last:
+                dot = jnp.square(jnp.maximum(dot, 0.0))
+            o_ref[rows, cols] = dot.astype(o_ref.dtype)
 
 
 def up_dot(own, oth, parts, acc=None, last=False):
-    more, n = acc is not None, len(parts)
-    rows, wide, tile = own.shape[0], parts[0][0].shape[1], 256
-    tokens, pieces, depth = [], [], 0
-    for p, at in parts:
-        k = p.shape[0]
-        tokens.append(pl.BlockSpec((rows, k), lambda j, i=at // k: (0, i)))
-        pieces.append(pl.BlockSpec((k, tile), lambda j: (0, j)))
-        depth += k
-    col = pl.BlockSpec((2 * rows, tile), lambda j: (0, j))
-    return pl.pallas_call(
-        functools.partial(up_kernel, n, more, last),
-        grid=(wide // tile,),
-        out_shape=jax.ShapeDtypeStruct((2 * rows, wide), jnp.bfloat16 if last else jnp.float32),
-        in_specs=tokens * 2 + pieces + ([col] if more else []),
-        out_specs=col,
+    rows, wide = 2 * own.shape[0], parts[0][0].shape[1]
+    depth = sum(p.shape[0] for p, _ in parts)
+    ins = (own, oth, *[p for p, _ in parts]) + (() if acc is None else (acc,))
+    places = tuple(at for _, at in parts)
+    return pl.pallas_call(
+        functools.partial(up_kernel, places, acc is not None, last),
+        out_shape=jax.ShapeDtypeStruct((rows, wide), jnp.bfloat16 if last else jnp.float32),
+        in_specs=[VMEM] * len(ins),
+        out_specs=VMEM,
         compiler_params=limit(24),
-        cost_estimate=cost(4 * rows * wide * depth, 6 * 2**20),
+        cost_estimate=cost(2 * rows * wide * depth, 6 * 2**20),
         name="up",
-    )(*[own] * n, *[oth] * n, *[p for p, _ in parts], *((acc,) if more else ()))
+    )(*ins)
 
 
 def down_kernel(first, h_ref, a_ref, b_ref, c_ref, d_ref, own_ref, oth_ref):
     half = h_ref.shape[0] // 2
-    rows = pl.ds(pl.multiple_of((pl.program_id(0) + first) * 64, 64), 64)
-    rhs = jnp.concatenate([r[rows, :] for r in (a_ref, b_ref, c_ref, d_ref)], axis=0)
-    for c, o_ref in enumerate((own_ref, oth_ref)):
-        cut = slice(c * half, (c + 1) * half)
-        o_ref[...] = lax.dot_general(
-            h_ref[cut, :], rhs, (((1,), (1,)), ((), ())), preferred_element_type=jnp.float32
-        ).astype(o_ref.dtype)
+
+    @pl.loop(0, own_ref.shape[1] // 256)
+    def _(j):
+        rows = pl.ds(pl.multiple_of((j + first) * 64, 64), 64)
+        cols = pl.ds(pl.multiple_of(j * 256, 256), 256)
+        rhs = jnp.concatenate([r[rows, :] for r in (a_ref, b_ref, c_ref, d_ref)], axis=0)
+        for c, o_ref in enumerate((own_ref, oth_ref)):
+            cut = slice(c * half, (c + 1) * half)
+            o_ref[:, cols] = lax.dot_general(
+                h_ref[cut, :], rhs, (((1,), (1,)), ((), ())), preferred_element_type=jnp.float32
+            ).astype(o_ref.dtype)
 
 
 def down_dot(hidden, parts, first, n):
-    rows, k = parts[0].shape
-    m, wide = hidden.shape
+    m, k = hidden.shape
     out = jax.ShapeDtypeStruct((m // 2, n * 256), jnp.bfloat16)
-    col = pl.BlockSpec((m // 2, 256), lambda j: (0, j))
     return pl.pallas_call(
         functools.partial(down_kernel, first),
-        grid=(n,),
         out_shape=(out, out),
-        in_specs=[pl.BlockSpec((m, wide), lambda j: (0, 0))]
-        + [pl.BlockSpec((rows, k), lambda j: (0, 0))] * NY,
-        out_specs=(col, col),
+        in_specs=[VMEM] * (1 + NY),
+        out_specs=(VMEM, VMEM),
         compiler_params=limit(24),
         cost_estimate=cost(2 * m * k * 256 * n, 6 * 2**20),
         name="down",

time: 174 us -> 174 us (level)
  Pallas kernels: 23.1 us -> 19.8 us
  waiting for transfers between devices: 91.6 us -> 94.7 us
    pallas_call x6, Pallas kernels: 15.8 us -> 12.5 us  [the longest x3 6.48 us: up_dot(): pl.pallas_call(functools.partial(up_kernel, places, acc is not None, last...]
    ppermute x40, waiting for transfers between devices: 91.6 us -> 94.7 us  [rot(): return lax.ppermute(v, axis, [(i, (i + by) % n) for i in range(n)])]
  transfers between devices with their start and end apart: 40 -> 40, of which waited for: 18 -> 18; matrix products, arithmetic and copies ran while one was open for 1% -> 1% of each run, Pallas kernels for 12% -> 11%
where the time goes in v2:
time: 174 us
  waiting for transfers between devices  94.7 us (54%)
  starting transfers between devices  55.8 us (32%)
  Pallas kernels  19.8 us (11%)
    ppermute x40, waiting for transfers between devices, rot(): return lax.ppermute(v, axis, [(i, (i + by) % n) for i in range(n)])  94.7 us
    ppermute x40, starting transfers between devices, rot(): return lax.ppermute(v, axis, [(i, (i + by) % n) for i in range(n)])  55.8 us
    pallas_call x3, Pallas kernels, up_dot(): pl.pallas_call(functools.partial(up_kernel, places, acc is not None, last...  6.48 us
    pallas_call x3, Pallas kernels, down_dot(): pl.pallas_call(functools.partial(down_kernel, first), out_shape=(out, out...  5.99 us
  transfers between devices with their start and end apart: 40, of which 18 were waited for; matrix products, arithmetic and copies ran while one was open for 1% of the time, Pallas kernels for 11%

profile of v2, /device:TPU:8, one launch (start us, length us, event | category | flops | bytes accessed | tf_op | source)
XLA Modules:
  0.0 174.0 jit_solution(7928649425601557668)
XLA Ops:
  0.6 1.0 copy-done
  1.9 2.8 %collective-permute-start.24 = (bf16[128,2048]{1,0:T(8,128)(2,1)S(1)}, bf16[128,2048]{1,0:T(8,128)(2,1)S(1)}, u32[]{:S(2)}, u32[]{:S(2)}) collective-permute-start(bf16[128,2048]{1,0:T(8,128)(2,1)S(1)} %norm.1.refs_0_), channel_id=1, source_target_pairs={{0,6},{2,0},{4,2},{6,4},{1,7},{3,1},{5,3},{7,5},{8,14},{10,8},{12,... | collective-permute-start | bytes 1572872 | tf_op jit(solution)/shard_map/ppermute | solution.py:20
  6.4 1.0 multiply_convert_fusion.refs_0_
  8.0 2.6 %collective-permute-start.1 = (bf16[64,1024]{1,0:T(8,128)(2,1)S(1)}, bf16[64,1024]{1,0:T(8,128)(2,1)S(1)}, u32[]{:S(2)}, u32[]{:S(2)}) collective-permute-start(bf16[64,1024]{1,0:T(8,128)(2,1)S(1)} %multiply_convert_fusion.refs_0_), channel_id=1, source_target_pairs={{0,16},{8,24},{16,0},{24,8},{1,17},{9,25},{17,1},{25,9},{2,18},{10... | collective-permute-start | bytes 393224 | tf_op jit(solution)/shard_map/ppermute | solution.py:20
  10.6 3.3 %collective-permute-done.refs_1_ = bf16[64,1024]{1,0:T(8,128)(2,1)S(1)} collective-permute-done((bf16[64,1024]{1,0:T(8,128)(2,1)S(1)}, bf16[64,1024]{1,0:T(8,128)(2,1)S(1)}, u32[]{:S(2)}, u32[]{:S(2)}) %collective-permute-start) | collective-permute-done | bytes 131104 | tf_op jit(solution)/shard_map/ppermute | solution.py:20
  13.9 1.0 collective-permute-start.2
  15.7 3.1 %collective-permute-done.2.refs_3_ = bf16[64,1024]{1,0:T(8,128)(2,1)S(1)} collective-permute-done((bf16[64,1024]{1,0:T(8,128)(2,1)S(1)}, bf16[64,1024]{1,0:T(8,128)(2,1)S(1)}, u32[]{:S(2)}, u32[]{:S(2)}) %collective-permute-start.2) | collective-permute-done | bytes 131104 | tf_op jit(solution)/shard_map/ppermute | solution.py:20
  19.6 2.0 %collective-permute-start.3 = (bf16[256,1024]{1,0:T(8,128)(2,1)S(1)}, bf16[256,1024]{1,0:T(8,128)(2,1)S(1)}, u32[]{:S(2)}, u32[]{:S(2)}) collective-permute-start(bf16[256,1024]{1,0:T(8,128)(2,1)S(1)} %place.3.refs_2_.refs_4_), channel_id=1, source_target_pairs={{0,32},{32,64},{64,96},{96,128},{128,160},{160,192},{192,224},{224... | collective-permute-start | bytes 1572872 | tf_op jit(solution)/shard_map/ppermute | solution.py:20
  21.6 5.6 %collective-permute-done.24.refs_1_ = bf16[128,2048]{1,0:T(8,128)(2,1)S(1)} collective-permute-done((bf16[128,2048]{1,0:T(8,128)(2,1)S(1)}, bf16[128,2048]{1,0:T(8,128)(2,1)S(1)}, u32[]{:S(2)}, u32[]{:S(2)}) %collective-permute-start.24) | collective-permute-done | bytes 524320 | tf_op jit(solution)/shard_map/ppermute | solution.py:20
  27.2 3.7 %collective-permute-done.26.refs_3_ = bf16[128,2048]{1,0:T(8,128)(2,1)S(1)} collective-permute-done((bf16[128,2048]{1,0:T(8,128)(2,1)S(1)}, bf16[128,2048]{1,0:T(8,128)(2,1)S(1)}, u32[]{:S(2)}, u32[]{:S(2)}) %collective-permute-start.26) | collective-permute-done | bytes 524320 | tf_op jit(solution)/shard_map/ppermute | solution.py:20
  31.1 5.9 %collective-permute-start.5 = (bf16[256,1024]{1,0:T(8,128)(2,1)S(1)}, bf16[256,1024]{1,0:T(8,128)(2,1)S(1)}, u32[]{:S(2)}, u32[]{:S(2)}) collective-permute-start(bf16[256,1024]{1,0:T(8,128)(2,1)S(1)} %place.3.refs_2_.refs_4_), channel_id=1, source_target_pairs={{0,224},{32,0},{64,32},{96,64},{128,96},{160,128},{192,160},{224,1... | collective-permute-start | bytes 1572872 | tf_op jit(solution)/shard_map/ppermute | solution.py:20
  37.1 3.3 %collective-permute-start.11 = (bf16[64,1024]{1,0:T(8,128)(2,1)S(1)}, bf16[64,1024]{1,0:T(8,128)(2,1)S(1)}, u32[]{:S(2)}, u32[]{:S(2)}) collective-permute-start(bf16[64,1024]{1,0:T(8,128)(2,1)S(1)} %get-tuple-element.16), channel_id=1, source_target_pairs={{0,224},{32,0},{64,32},{96,64},{128,96},{160,128},{192,160},{224,1... | collective-permute-start | bytes 393224 | tf_op jit(solution)/shard_map/ppermute | solution.py:20
  40.4 11.2 %collective-permute-done.11 = bf16[64,1024]{1,0:T(8,128)(2,1)S(1)} collective-permute-done((bf16[64,1024]{1,0:T(8,128)(2,1)S(1)}, bf16[64,1024]{1,0:T(8,128)(2,1)S(1)}, u32[]{:S(2)}, u32[]{:S(2)}) %collective-permute-start.11) | collective-permute-done | bytes 131104 | tf_op jit(solution)/shard_map/ppermute | solution.py:20
  51.6 2.9 %collective-permute-start.13 = (bf16[64,1024]{1,0:T(8,128)(2,1)S(1)}, bf16[64,1024]{1,0:T(8,128)(2,1)S(1)}, u32[]{:S(2)}, u32[]{:S(2)}) collective-permute-start(bf16[64,1024]{1,0:T(8,128)(2,1)S(1)} %get-tuple-element.16), channel_id=1, source_target_pairs={{0,192},{32,224},{64,0},{96,32},{128,64},{160,96},{192,128},{224,1... | collective-permute-start | bytes 393224 | tf_op jit(solution)/shard_map/ppermute | solution.py:20
  54.6 1.0 collective-permute-start.6
  55.6 2.8 %collective-permute-start.14 = (bf16[64,1024]{1,0:T(8,128)(2,1)S(1)}, bf16[64,1024]{1,0:T(8,128)(2,1)S(1)}, u32[]{:S(2)}, u32[]{:S(2)}) collective-permute-start(bf16[64,1024]{1,0:T(8,128)(2,1)S(1)} %get-tuple-element.16), channel_id=1, source_target_pairs={{0,64},{32,96},{64,128},{96,160},{128,192},{160,224},{192,0},{224,... | collective-permute-start | bytes 393224 | tf_op jit(solution)/shard_map/ppermute | solution.py:20
  58.4 2.7 %collective-permute-done.13 = bf16[64,1024]{1,0:T(8,128)(2,1)S(1)} collective-permute-done((bf16[64,1024]{1,0:T(8,128)(2,1)S(1)}, bf16[64,1024]{1,0:T(8,128)(2,1)S(1)}, u32[]{:S(2)}, u32[]{:S(2)}) %collective-permute-start.13) | collective-permute-done | bytes 131104 | tf_op jit(solution)/shard_map/ppermute | solution.py:20
  61.1 1.0 collective-permute-start.7
  62.1 2.2 %collective-permute-done.14 = bf16[64,1024]{1,0:T(8,128)(2,1)S(1)} collective-permute-done((bf16[64,1024]{1,0:T(8,128)(2,1)S(1)}, bf16[64,1024]{1,0:T(8,128)(2,1)S(1)}, u32[]{:S(2)}, u32[]{:S(2)}) %collective-permute-start.14) | collective-permute-done | bytes 131104 | tf_op jit(solution)/shard_map/ppermute | solution.py:20
  65.1 7.5 %collective-permute-done.6.refs_4_.refs_6_ = bf16[256,1024]{1,0:T(8,128)(2,1)S(1)} collective-permute-done((bf16[256,1024]{1,0:T(8,128)(2,1)S(1)}, bf16[256,1024]{1,0:T(8,128)(2,1)S(1)}, u32[]{:S(2)}, u32[]{:S(2)}) %collective-permute-start.6) | collective-permute-done | bytes 524320 | tf_op jit(solution)/shard_map/ppermute | solution.py:20
  72.6 2.2 %collective-permute-start.8 = (bf16[256,1024]{1,0:T(8,128)(2,1)S(1)}, bf16[256,1024]{1,0:T(8,128)(2,1)S(1)}, u32[]{:S(2)}, u32[]{:S(2)}) collective-permute-start(bf16[256,1024]{1,0:T(8,128)(2,1)S(1)} %collective-permute-done.6.refs_4_.refs_6_), channel_id=1, source_target_pairs={{0,224},{32,0},{64,32},{96,64},{128,96},{160,128},{192,160},{224,1... | collective-permute-start | bytes 1572872 | tf_op jit(solution)/shard_map/ppermute | solution.py:20
  74.8 14.3 %collective-permute-done.18 = bf16[64,1024]{1,0:T(8,128)(2,1)S(1)} collective-permute-done((bf16[64,1024]{1,0:T(8,128)(2,1)S(1)}, bf16[64,1024]{1,0:T(8,128)(2,1)S(1)}, u32[]{:S(2)}, u32[]{:S(2)}) %collective-permute-start.18) | collective-permute-done | bytes 131104 | tf_op jit(solution)/shard_map/ppermute | solution.py:20
  89.1 3.2 %collective-permute-start.20 = (bf16[64,1024]{1,0:T(8,128)(2,1)S(1)}, bf16[64,1024]{1,0:T(8,128)(2,1)S(1)}, u32[]{:S(2)}, u32[]{:S(2)}) collective-permute-start(bf16[64,1024]{1,0:T(8,128)(2,1)S(1)} %collective-permute-done.18), channel_id=1, source_target_pairs={{0,224},{32,0},{64,32},{96,64},{128,96},{160,128},{192,160},{224,1... | collective-permute-start | bytes 393224 | tf_op jit(solution)/shard_map/ppermute | solution.py:20
  92.4 2.4 %collective-permute-start.16 = (bf16[320,1024]{1,0:T(8,128)(2,1)S(1)}, bf16[320,1024]{1,0:T(8,128)(2,1)S(1)}, u32[]{:S(2)}, u32[]{:S(2)}) collective-permute-start(bf16[320,1024]{1,0:T(8,128)(2,1)S(1)} %constant_dynamic-update-slice_fusion.refs_0_.a_ref), channel_id=1, source_target_pairs={{0,16},{8,24},{16,0},{24,8},{1,17},{9,25},{17,1},{25,9},{2,18},{10... | collective-permute-start | bytes 1966088 | tf_op jit(solution)/shard_map/ppermute | solution.py:20
  95.3 1.6 collective-permute-start.17
  96.9 3.2 %collective-permute-start.9 = (bf16[128,1024]{1,0:T(8,128)(2,1)S(1)}, bf16[128,1024]{1,0:T(8,128)(2,1)S(1)}, u32[]{:S(2)}, u32[]{:S(2)}) collective-permute-start(bf16[128,1024]{1,0:T(8,128)(2,1)S(1)} %slice.56), channel_id=1, source_target_pairs={{0,224},{32,0},{64,32},{96,64},{128,96},{160,128},{192,160},{224,1... | collective-permute-start | bytes 786440 | tf_op jit(solution)/shard_map/ppermute | solution.py:20
  100.2 4.3 %collective-permute-done.10.refs_8_.refs_3_ = bf16[128,1024]{1,0:T(8,128)(2,1)S(1)} collective-permute-done((bf16[128,1024]{1,0:T(8,128)(2,1)S(1)}, bf16[128,1024]{1,0:T(8,128)(2,1)S(1)}, u32[]{:S(2)}, u32[]{:S(2)}) %collective-permute-start.10) | collective-permute-done | bytes 262176 | tf_op jit(solution)/shard_map/ppermute | solution.py:20
  104.9 2.3 %collective-permute-start.22 = (bf16[192,1024]{1,0:T(8,128)(2,1)S(1)}, bf16[192,1024]{1,0:T(8,128)(2,1)S(1)}, u32[]{:S(2)}, u32[]{:S(2)}) collective-permute-start(bf16[192,1024]{1,0:T(8,128)(2,1)S(1)} %constant_dynamic-update-slice_fusion.5.refs_4_.a_ref), channel_id=1, source_target_pairs={{0,16},{8,24},{16,0},{24,8},{1,17},{9,25},{17,1},{25,9},{2,18},{10... | collective-permute-start | bytes 1179656 | tf_op jit(solution)/shard_map/ppermute | solution.py:20
  107.2 1.3 collective-permute-start.23
  108.5 3.4 %up.3.refs_4_ = f32[1024,1024]{1,0:T(8,128)S(1)} custom-call(bf16[512,2048]{1,0:T(8,128)(2,1)S(1)} %place.5.refs_0_, bf16[512,2048]{1,0:T(8,128)(2,1)S(1)} %collective-permute-done.27.refs_1_, bf16[256,1024]{1,0:T(8,128)(2,1)S(1)} %collective-permute-done.4.refs_0_.refs_2_, bf16[256,1024]{1,0:T(8,128)(2,1)S(1)} %collective-permute-done.3.refs_1_.refs_3_, ...), custom_call_target="tpu_custom_call" | custom-call | flops 2684354560 | bytes 6291456 | tf_op jit(solution)/shard_map/up/pallas_call | solution.py:108
  111.9 1.8 %up.4.refs_4_ = f32[1024,1024]{1,0:T(8,128)S(1)} custom-call(bf16[512,2048]{1,0:T(8,128)(2,1)S(1)} %place.5.refs_0_, bf16[512,2048]{1,0:T(8,128)(2,1)S(1)} %collective-permute-done.27.refs_1_, bf16[256,1024]{1,0:T(8,128)(2,1)S(1)} %collective-permute-done.7.refs_5_.refs_2_, bf16[256,1024]{1,0:T(8,128)(2,1)S(1)} %collective-permute-done.8.refs_6_.refs_3_, ...), custom_call_target="tpu_custom_call" | custom-call | flops 1073741824 | bytes 6291456 | tf_op jit(solution)/shard_map/up/pallas_call | solution.py:108
  113.7 1.3 up.5.h_ref
  115.0 10.7 %collective-permute-done.17.refs_3_.d_ref = bf16[320,1024]{1,0:T(8,128)(2,1)S(1)} collective-permute-done((bf16[320,1024]{1,0:T(8,128)(2,1)S(1)}, bf16[320,1024]{1,0:T(8,128)(2,1)S(1)}, u32[]{:S(2)}, u32[]{:S(2)}) %collective-permute-start.17) | collective-permute-done | bytes 655392 | tf_op jit(solution)/shard_map/ppermute | solution.py:20
  125.7 1.5 down.3
  127.4 12.8 %collective-permute-done.23.refs_7_.d_ref = bf16[192,1024]{1,0:T(8,128)(2,1)S(1)} collective-permute-done((bf16[192,1024]{1,0:T(8,128)(2,1)S(1)}, bf16[192,1024]{1,0:T(8,128)(2,1)S(1)}, u32[]{:S(2)}, u32[]{:S(2)}) %collective-permute-start.23) | collective-permute-done | bytes 393248 | tf_op jit(solution)/shard_map/ppermute | solution.py:20
  140.1 2.3 %down.5 = (bf16[512,768]{1,0:T(8,128)(2,1)S(1)}, bf16[512,768]{1,0:T(8,128)(2,1)S(1)}) custom-call(bf16[1024,1024]{1,0:T(8,128)(2,1)S(1)} %up.5.h_ref, bf16[192,1024]{1,0:T(8,128)(2,1)S(1)} %constant_dynamic-update-slice_fusion.5.refs_4_.a_ref, bf16[192,1024]{1,0:T(8,128)(2,1)S(1)} %collective-permute-done.21.refs_5_.b_ref, ...), custom_call_target="tpu_custom_call" | custom-call | flops 1610612736 | bytes 6291456 | tf_op jit(solution)/shard_map/down/pallas_call | solution.py:137
  142.5 2.2 %down.4 = (bf16[512,768]{1,0:T(8,128)(2,1)S(1)}, bf16[512,768]{1,0:T(8,128)(2,1)S(1)}) custom-call(bf16[1024,1024]{1,0:T(8,128)(2,1)S(1)} %up.5.h_ref, bf16[320,1024]{1,0:T(8,128)(2,1)S(1)} %constant_dynamic-update-slice_fusion.refs_0_.a_ref, bf16[320,1024]{1,0:T(8,128)(2,1)S(1)} %collective-permute-done.15.refs_1_.b_ref, ...), custom_call_target="tpu_custom_call" | custom-call | flops 1610612736 | bytes 6291456 | tf_op jit(solution)/shard_map/down/pallas_call | solution.py:137
  145.9 2.0 %collective-permute-start.30 = (bf16[128,512]{1,0:T(8,128)(2,1)S(1)}, bf16[128,512]{1,0:T(8,128)(2,1)S(1)}, u32[]{:S(2)}, u32[]{:S(2)}) collective-permute-start(bf16[128,512]{1,0:T(8,128)(2,1)S(1)} %get-tuple-element.26), channel_id=1, source_target_pairs={{0,4},{2,6},{4,0},{6,2},{1,5},{3,7},{5,1},{7,3},{8,12},{10,14},{12... | collective-permute-start | bytes 393224 | tf_op jit(solution)/shard_map/ppermute | solution.py:20
  147.9 1.3 collective-permute-start.31
  150.3 2.2 %collective-permute-start.38 = (bf16[128,768]{1,0:T(8,128)(2,1)S(1)}, bf16[128,768]{1,0:T(8,128)(2,1)S(1)}, u32[]{:S(2)}, u32[]{:S(2)}) collective-permute-start(bf16[128,768]{1,0:T(8,128)(2,1)S(1)} %get-tuple-element.18), channel_id=1, source_target_pairs={{0,4},{2,6},{4,0},{6,2},{1,5},{3,7},{5,1},{7,3},{8,12},{10,14},{12... | collective-permute-start | bytes 589832 | tf_op jit(solution)/shard_map/ppermute | solution.py:20
  152.7 3.4 %collective-permute-done.29.refs_1_ = bf16[128,512]{1,0:T(8,128)(2,1)S(1)} collective-permute-done((bf16[128,512]{1,0:T(8,128)(2,1)S(1)}, bf16[128,512]{1,0:T(8,128)(2,1)S(1)}, u32[]{:S(2)}, u32[]{:S(2)}) %collective-permute-start.29) | collective-permute-done | bytes 131104 | tf_op jit(solution)/shard_map/ppermute | solution.py:20
  156.1 2.0 %collective-permute-start.33 = (bf16[128,768]{1,0:T(8,128)(2,1)S(1)}, bf16[128,768]{1,0:T(8,128)(2,1)S(1)}, u32[]{:S(2)}, u32[]{:S(2)}) collective-permute-start(bf16[128,768]{1,0:T(8,128)(2,1)S(1)} %get-tuple-element.23), channel_id=1, source_target_pairs={{0,2},{2,4},{4,6},{6,0},{1,3},{3,5},{5,7},{7,1},{8,10},{10,12},{12... | collective-permute-start | bytes 589832 | tf_op jit(solution)/shard_map/ppermute | solution.py:20
  158.1 1.3 collective-permute-start.34
  159.4 5.1 %collective-permute-done.37.refs_9_ = bf16[128,768]{1,0:T(8,128)(2,1)S(1)} collective-permute-done((bf16[128,768]{1,0:T(8,128)(2,1)S(1)}, bf16[128,768]{1,0:T(8,128)(2,1)S(1)}, u32[]{:S(2)}, u32[]{:S(2)}) %collective-permute-start.37) | collective-permute-done | bytes 196640 | tf_op jit(solution)/shard_map/ppermute | solution.py:20
  164.5 2.9 %turn.1 = bf16[1024,2048]{1,0:T(8,128)(2,1)} custom-call(bf16[320,1024]{1,0:T(8,128)(2,1)S(1)} %constant_dynamic-update-slice_fusion.refs_0_.a_ref, bf16[320,1024]{1,0:T(8,128)(2,1)S(1)} %collective-permute-done.15.refs_1_.b_ref, bf16[320,1024]{1,0:T(8,128)(2,1)S(1)} %collective-permute-done.16.refs_2_.c_ref, ...), custom_call_target="tpu_custom_call" | custom-call | flops 2000000000 | bytes 8388608 | tf_op jit(solution)/shard_map/turn/pallas_call | solution.py:177
  167.5 2.1 %place.4 = bf16[2048,1024]{1,0:T(8,128)(2,1)} custom-call(bf16[256,1024]{1,0:T(8,128)(2,1)S(1)} %collective-permute-done.4.refs_0_.refs_2_, bf16[256,1024]{1,0:T(8,128)(2,1)S(1)} %collective-permute-done.3.refs_1_.refs_3_, bf16[256,1024]{1,0:T(8,128)(2,1)S(1)} %place.3.refs_2_.refs_4_, bf16[256,1024]{1,0:T(8,128)(2,1)S(1)} %collective-permute-done.5.refs_3_.refs_5_, ...), custom_call_target="tpu_custom_call" | custom-call | tf_op jit(solution)/shard_map/place/pallas_call | solution.py:71
  169.6 2.6 %collective-permute-done.33.refs_5_ = bf16[128,768]{1,0:T(8,128)(2,1)S(1)} collective-permute-done((bf16[128,768]{1,0:T(8,128)(2,1)S(1)}, bf16[128,768]{1,0:T(8,128)(2,1)S(1)}, u32[]{:S(2)}, u32[]{:S(2)}) %collective-permute-start.33) | collective-permute-done | bytes 196640 | tf_op jit(solution)/shard_map/ppermute | solution.py:20
  172.8 1.2 total.1
  (65 shorter events, 9.3 us)
Async XLA Ops:
  0.6 1.0 copy-start
  1.9 25.3 %collective-permute-start.24 = (bf16[128,2048]{1,0:T(8,128)(2,1)S(1)}, bf16[128,2048]{1,0:T(8,128)(2,1)S(1)}, u32[]{:S(2)}, u32[]{:S(2)}) collective-permute-start(bf16[128,2048]{1,0:T(8,128)(2,1)S(1)} %norm.1.refs_0_), channel_id=1, source_target_pairs={{0,6},{2,0},{4,2},{6,4},{1,7},{3,1},{5,3},{7,5},{8,14},{10,8},{12,... | collective-permute-start | bytes 1572872 | tf_op jit(solution)/shard_map/ppermute | solution.py:20
  4.7 22.5 %collective-permute-start.25 = (bf16[128,2048]{1,0:T(8,128)(2,1)S(1)}, bf16[128,2048]{1,0:T(8,128)(2,1)S(1)}, u32[]{:S(2)}, u32[]{:S(2)}) collective-permute-start(bf16[128,2048]{1,0:T(8,128)(2,1)S(1)} %norm.1.refs_0_), channel_id=1, source_target_pairs={{0,4},{2,6},{4,0},{6,2},{1,5},{3,7},{5,1},{7,3},{8,12},{10,14},{12... | collective-permute-start | bytes 1572872 | tf_op jit(solution)/shard_map/ppermute | solution.py:20
  5.5 25.3 %collective-permute-start.26 = (bf16[128,2048]{1,0:T(8,128)(2,1)S(1)}, bf16[128,2048]{1,0:T(8,128)(2,1)S(1)}, u32[]{:S(2)}, u32[]{:S(2)}) collective-permute-start(bf16[128,2048]{1,0:T(8,128)(2,1)S(1)} %norm.1.refs_0_), channel_id=1, source_target_pairs={{0,2},{2,4},{4,6},{6,0},{1,3},{3,5},{5,7},{7,1},{8,10},{10,12},{12... | collective-permute-start | bytes 1572872 | tf_op jit(solution)/shard_map/ppermute | solution.py:20
  7.4 6.4 %collective-permute-start = (bf16[64,1024]{1,0:T(8,128)(2,1)S(1)}, bf16[64,1024]{1,0:T(8,128)(2,1)S(1)}, u32[]{:S(2)}, u32[]{:S(2)}) collective-permute-start(bf16[64,1024]{1,0:T(8,128)(2,1)S(1)} %multiply_convert_fusion.refs_0_), channel_id=1, source_target_pairs={{0,24},{8,0},{16,8},{24,16},{1,25},{9,1},{17,9},{25,17},{2,26},{10... | collective-permute-start | bytes 393224 | tf_op jit(solution)/shard_map/ppermute | solution.py:20
  8.0 7.8 %collective-permute-start.1 = (bf16[64,1024]{1,0:T(8,128)(2,1)S(1)}, bf16[64,1024]{1,0:T(8,128)(2,1)S(1)}, u32[]{:S(2)}, u32[]{:S(2)}) collective-permute-start(bf16[64,1024]{1,0:T(8,128)(2,1)S(1)} %multiply_convert_fusion.refs_0_), channel_id=1, source_target_pairs={{0,16},{8,24},{16,0},{24,8},{1,17},{9,25},{17,1},{25,9},{2,18},{10... | collective-permute-start | bytes 393224 | tf_op jit(solution)/shard_map/ppermute | solution.py:20
  13.9 5.0 %collective-permute-start.2 = (bf16[64,1024]{1,0:T(8,128)(2,1)S(1)}, bf16[64,1024]{1,0:T(8,128)(2,1)S(1)}, u32[]{:S(2)}, u32[]{:S(2)}) collective-permute-start(bf16[64,1024]{1,0:T(8,128)(2,1)S(1)} %multiply_convert_fusion.refs_0_), channel_id=1, source_target_pairs={{0,8},{8,16},{16,24},{24,0},{1,9},{9,17},{17,25},{25,1},{2,10},{10... | collective-permute-start | bytes 393224 | tf_op jit(solution)/shard_map/ppermute | solution.py:20
  19.6 17.5 %copy-start.1 = (f32[64,1024]{1,0:T(8,128)S(1)}, f32[64,1024]{1,0:T(8,128)}, u32[]{:S(2)}) copy-start(f32[64,1024]{1,0:T(8,128)} %param.7) | copy-start | bytes 786436
  19.6 17.5 %collective-permute-start.3 = (bf16[256,1024]{1,0:T(8,128)(2,1)S(1)}, bf16[256,1024]{1,0:T(8,128)(2,1)S(1)}, u32[]{:S(2)}, u32[]{:S(2)}) collective-permute-start(bf16[256,1024]{1,0:T(8,128)(2,1)S(1)} %place.3.refs_2_.refs_4_), channel_id=1, source_target_pairs={{0,32},{32,64},{64,96},{96,128},{128,160},{160,192},{192,224},{224... | collective-permute-start | bytes 1572872 | tf_op jit(solution)/shard_map/ppermute | solution.py:20
  31.0 76.2 %collective-permute-start.27 = (bf16[512,2048]{1,0:T(8,128)(2,1)S(1)}, bf16[512,2048]{1,0:T(8,128)(2,1)S(1)}, u32[]{:S(2)}, u32[]{:S(2)}) collective-permute-start(bf16[512,2048]{1,0:T(8,128)(2,1)S(1)} %place.5.refs_0_), channel_id=1, source_target_pairs={{0,1},{1,0},{2,3},{3,2},{4,5},{5,4},{6,7},{7,6},{8,9},{9,8},{10,11... | collective-permute-start | bytes 6291464 | tf_op jit(solution)/shard_map/ppermute | solution.py:20
  31.1 23.4 %collective-permute-start.5 = (bf16[256,1024]{1,0:T(8,128)(2,1)S(1)}, bf16[256,1024]{1,0:T(8,128)(2,1)S(1)}, u32[]{:S(2)}, u32[]{:S(2)}) collective-permute-start(bf16[256,1024]{1,0:T(8,128)(2,1)S(1)} %place.3.refs_2_.refs_4_), channel_id=1, source_target_pairs={{0,224},{32,0},{64,32},{96,64},{128,96},{160,128},{192,160},{224,1... | collective-permute-start | bytes 1572872 | tf_op jit(solution)/shard_map/ppermute | solution.py:20
  37.1 24.1 %collective-permute-start.4 = (bf16[256,1024]{1,0:T(8,128)(2,1)S(1)}, bf16[256,1024]{1,0:T(8,128)(2,1)S(1)}, u32[]{:S(2)}, u32[]{:S(2)}) collective-permute-start(bf16[256,1024]{1,0:T(8,128)(2,1)S(1)} %collective-permute-done.3.refs_1_.refs_3_), channel_id=1, source_target_pairs={{0,32},{32,64},{64,96},{96,128},{128,160},{160,192},{192,224},{224... | collective-permute-start | bytes 1572872 | tf_op jit(solution)/shard_map/ppermute | solution.py:20
  37.1 14.5 %collective-permute-start.11 = (bf16[64,1024]{1,0:T(8,128)(2,1)S(1)}, bf16[64,1024]{1,0:T(8,128)(2,1)S(1)}, u32[]{:S(2)}, u32[]{:S(2)}) collective-permute-start(bf16[64,1024]{1,0:T(8,128)(2,1)S(1)} %get-tuple-element.16), channel_id=1, source_target_pairs={{0,224},{32,0},{64,32},{96,64},{128,96},{160,128},{192,160},{224,1... | collective-permute-start | bytes 393224 | tf_op jit(solution)/shard_map/ppermute | solution.py:20
  40.4 15.2 %collective-permute-start.12 = (bf16[64,1024]{1,0:T(8,128)(2,1)S(1)}, bf16[64,1024]{1,0:T(8,128)(2,1)S(1)}, u32[]{:S(2)}, u32[]{:S(2)}) collective-permute-start(bf16[64,1024]{1,0:T(8,128)(2,1)S(1)} %get-tuple-element.16), channel_id=1, source_target_pairs={{0,32},{32,64},{64,96},{96,128},{128,160},{160,192},{192,224},{224... | collective-permute-start | bytes 393224 | tf_op jit(solution)/shard_map/ppermute | solution.py:20
  51.6 9.5 %collective-permute-start.13 = (bf16[64,1024]{1,0:T(8,128)(2,1)S(1)}, bf16[64,1024]{1,0:T(8,128)(2,1)S(1)}, u32[]{:S(2)}, u32[]{:S(2)}) collective-permute-start(bf16[64,1024]{1,0:T(8,128)(2,1)S(1)} %get-tuple-element.16), channel_id=1, source_target_pairs={{0,192},{32,224},{64,0},{96,32},{128,64},{160,96},{192,128},{224,1... | collective-permute-start | bytes 393224 | tf_op jit(solution)/shard_map/ppermute | solution.py:20
  54.6 18.0 %collective-permute-start.6 = (bf16[256,1024]{1,0:T(8,128)(2,1)S(1)}, bf16[256,1024]{1,0:T(8,128)(2,1)S(1)}, u32[]{:S(2)}, u32[]{:S(2)}) collective-permute-start(bf16[256,1024]{1,0:T(8,128)(2,1)S(1)} %collective-permute-done.5.refs_3_.refs_5_), channel_id=1, source_target_pairs={{0,224},{32,0},{64,32},{96,64},{128,96},{160,128},{192,160},{224,1... | collective-permute-start | bytes 1572872 | tf_op jit(solution)/shard_map/ppermute | solution.py:20
  55.6 8.8 %collective-permute-start.14 = (bf16[64,1024]{1,0:T(8,128)(2,1)S(1)}, bf16[64,1024]{1,0:T(8,128)(2,1)S(1)}, u32[]{:S(2)}, u32[]{:S(2)}) collective-permute-start(bf16[64,1024]{1,0:T(8,128)(2,1)S(1)} %get-tuple-element.16), channel_id=1, source_target_pairs={{0,64},{32,96},{64,128},{96,160},{128,192},{160,224},{192,0},{224,... | collective-permute-start | bytes 393224 | tf_op jit(solution)/shard_map/ppermute | solution.py:20
  61.1 28.0 %collective-permute-start.7 = (bf16[256,1024]{1,0:T(8,128)(2,1)S(1)}, bf16[256,1024]{1,0:T(8,128)(2,1)S(1)}, u32[]{:S(2)}, u32[]{:S(2)}) collective-permute-start(bf16[256,1024]{1,0:T(8,128)(2,1)S(1)} %collective-permute-done.4.refs_0_.refs_2_), channel_id=1, source_target_pairs={{0,32},{32,64},{64,96},{96,128},{128,160},{160,192},{192,224},{224... | collective-permute-start | bytes 1572872 | tf_op jit(solution)/shard_map/ppermute | solution.py:20
  64.4 32.5 %collective-permute-start.15 = (bf16[320,1024]{1,0:T(8,128)(2,1)S(1)}, bf16[320,1024]{1,0:T(8,128)(2,1)S(1)}, u32[]{:S(2)}, u32[]{:S(2)}) collective-permute-start(bf16[320,1024]{1,0:T(8,128)(2,1)S(1)} %constant_dynamic-update-slice_fusion.refs_0_.a_ref), channel_id=1, source_target_pairs={{0,24},{8,0},{16,8},{24,16},{1,25},{9,1},{17,9},{25,17},{2,26},{10... | collective-permute-start | bytes 1966088 | tf_op jit(solution)/shard_map/ppermute | solution.py:20
  72.6 19.8 %collective-permute-start.8 = (bf16[256,1024]{1,0:T(8,128)(2,1)S(1)}, bf16[256,1024]{1,0:T(8,128)(2,1)S(1)}, u32[]{:S(2)}, u32[]{:S(2)}) collective-permute-start(bf16[256,1024]{1,0:T(8,128)(2,1)S(1)} %collective-permute-done.6.refs_4_.refs_6_), channel_id=1, source_target_pairs={{0,224},{32,0},{64,32},{96,64},{128,96},{160,128},{192,160},{224,1... | collective-permute-start | bytes 1572872 | tf_op jit(solution)/shard_map/ppermute | solution.py:20
  74.8 14.3 %collective-permute-start.18 = (bf16[64,1024]{1,0:T(8,128)(2,1)S(1)}, bf16[64,1024]{1,0:T(8,128)(2,1)S(1)}, u32[]{:S(2)}, u32[]{:S(2)}) collective-permute-start(bf16[64,1024]{1,0:T(8,128)(2,1)S(1)} %collective-permute-done.13), channel_id=1, source_target_pairs={{0,224},{32,0},{64,32},{96,64},{128,96},{160,128},{192,160},{224,1... | collective-permute-start | bytes 393224 | tf_op jit(solution)/shard_map/ppermute | solution.py:20
  89.1 6.2 %collective-permute-start.19 = (bf16[64,1024]{1,0:T(8,128)(2,1)S(1)}, bf16[64,1024]{1,0:T(8,128)(2,1)S(1)}, u32[]{:S(2)}, u32[]{:S(2)}) collective-permute-start(bf16[64,1024]{1,0:T(8,128)(2,1)S(1)} %collective-permute-done.14), channel_id=1, source_target_pairs={{0,32},{32,64},{64,96},{96,128},{128,160},{160,192},{192,224},{224... | collective-permute-start | bytes 393224 | tf_op jit(solution)/shard_map/ppermute | solution.py:20
  89.1 7.8 %collective-permute-start.20 = (bf16[64,1024]{1,0:T(8,128)(2,1)S(1)}, bf16[64,1024]{1,0:T(8,128)(2,1)S(1)}, u32[]{:S(2)}, u32[]{:S(2)}) collective-permute-start(bf16[64,1024]{1,0:T(8,128)(2,1)S(1)} %collective-permute-done.18), channel_id=1, source_target_pairs={{0,224},{32,0},{64,32},{96,64},{128,96},{160,128},{192,160},{224,1... | collective-permute-start | bytes 393224 | tf_op jit(solution)/shard_map/ppermute | solution.py:20
  92.4 22.6 %collective-permute-start.16 = (bf16[320,1024]{1,0:T(8,128)(2,1)S(1)}, bf16[320,1024]{1,0:T(8,128)(2,1)S(1)}, u32[]{:S(2)}, u32[]{:S(2)}) collective-permute-start(bf16[320,1024]{1,0:T(8,128)(2,1)S(1)} %constant_dynamic-update-slice_fusion.refs_0_.a_ref), channel_id=1, source_target_pairs={{0,16},{8,24},{16,0},{24,8},{1,17},{9,25},{17,1},{25,9},{2,18},{10... | collective-permute-start | bytes 1966088 | tf_op jit(solution)/shard_map/ppermute | solution.py:20
  95.3 30.5 %collective-permute-start.17 = (bf16[320,1024]{1,0:T(8,128)(2,1)S(1)}, bf16[320,1024]{1,0:T(8,128)(2,1)S(1)}, u32[]{:S(2)}, u32[]{:S(2)}) collective-permute-start(bf16[320,1024]{1,0:T(8,128)(2,1)S(1)} %constant_dynamic-update-slice_fusion.refs_0_.a_ref), channel_id=1, source_target_pairs={{0,8},{8,16},{16,24},{24,0},{1,9},{9,17},{17,25},{25,1},{2,10},{10... | collective-permute-start | bytes 1966088 | tf_op jit(solution)/shard_map/ppermute | solution.py:20
  96.9 7.6 %collective-permute-start.10 = (bf16[128,1024]{1,0:T(8,128)(2,1)S(1)}, bf16[128,1024]{1,0:T(8,128)(2,1)S(1)}, u32[]{:S(2)}, u32[]{:S(2)}) collective-permute-start(bf16[128,1024]{1,0:T(8,128)(2,1)S(1)} %slice.57), channel_id=1, source_target_pairs={{0,32},{32,64},{64,96},{96,128},{128,160},{160,192},{192,224},{224... | collective-permute-start | bytes 786440 | tf_op jit(solution)/shard_map/ppermute | solution.py:20
  96.9 8.0 %collective-permute-start.9 = (bf16[128,1024]{1,0:T(8,128)(2,1)S(1)}, bf16[128,1024]{1,0:T(8,128)(2,1)S(1)}, u32[]{:S(2)}, u32[]{:S(2)}) collective-permute-start(bf16[128,1024]{1,0:T(8,128)(2,1)S(1)} %slice.56), channel_id=1, source_target_pairs={{0,224},{32,0},{64,32},{96,64},{128,96},{160,128},{192,160},{224,1... | collective-permute-start | bytes 786440 | tf_op jit(solution)/shard_map/ppermute | solution.py:20
  104.4 22.9 %collective-permute-start.21 = (bf16[192,1024]{1,0:T(8,128)(2,1)S(1)}, bf16[192,1024]{1,0:T(8,128)(2,1)S(1)}, u32[]{:S(2)}, u32[]{:S(2)}) collective-permute-start(bf16[192,1024]{1,0:T(8,128)(2,1)S(1)} %constant_dynamic-update-slice_fusion.5.refs_4_.a_ref), channel_id=1, source_target_pairs={{0,24},{8,0},{16,8},{24,16},{1,25},{9,1},{17,9},{25,17},{2,26},{10... | collective-permute-start | bytes 1179656 | tf_op jit(solution)/shard_map/ppermute | solution.py:20
  104.9 22.5 %collective-permute-start.22 = (bf16[192,1024]{1,0:T(8,128)(2,1)S(1)}, bf16[192,1024]{1,0:T(8,128)(2,1)S(1)}, u32[]{:S(2)}, u32[]{:S(2)}) collective-permute-start(bf16[192,1024]{1,0:T(8,128)(2,1)S(1)} %constant_dynamic-update-slice_fusion.5.refs_4_.a_ref), channel_id=1, source_target_pairs={{0,16},{8,24},{16,0},{24,8},{1,17},{9,25},{17,1},{25,9},{2,18},{10... | collective-permute-start | bytes 1179656 | tf_op jit(solution)/shard_map/ppermute | solution.py:20
  107.2 32.9 %collective-permute-start.23 = (bf16[192,1024]{1,0:T(8,128)(2,1)S(1)}, bf16[192,1024]{1,0:T(8,128)(2,1)S(1)}, u32[]{:S(2)}, u32[]{:S(2)}) collective-permute-start(bf16[192,1024]{1,0:T(8,128)(2,1)S(1)} %constant_dynamic-update-slice_fusion.5.refs_4_.a_ref), channel_id=1, source_target_pairs={{0,8},{8,16},{16,24},{24,0},{1,9},{9,17},{17,25},{25,1},{2,10},{10... | collective-permute-start | bytes 1179656 | tf_op jit(solution)/shard_map/ppermute | solution.py:20
  127.2 18.3 %collective-permute-start.28 = (bf16[512,512]{1,0:T(8,128)(2,1)S(1)}, bf16[512,512]{1,0:T(8,128)(2,1)S(1)}, u32[]{:S(2)}, u32[]{:S(2)}) collective-permute-start(bf16[512,512]{1,0:T(8,128)(2,1)S(1)} %get-tuple-element.10), channel_id=1, source_target_pairs={{0,1},{1,0},{2,3},{3,2},{4,5},{5,4},{6,7},{7,6},{8,9},{9,8},{10,11... | collective-permute-start | bytes 1572872 | tf_op jit(solution)/shard_map/ppermute | solution.py:20
  142.4 6.8 %collective-permute-start.36 = (bf16[512,768]{1,0:T(8,128)(2,1)S(1)}, bf16[512,768]{1,0:T(8,128)(2,1)S(1)}, u32[]{:S(2)}, u32[]{:S(2)}) collective-permute-start(bf16[512,768]{1,0:T(8,128)(2,1)S(1)} %get-tuple-element.14), channel_id=1, source_target_pairs={{0,1},{1,0},{2,3},{3,2},{4,5},{5,4},{6,7},{7,6},{8,9},{9,8},{10,11... | collective-permute-start | bytes 2359304 | tf_op jit(solution)/shard_map/ppermute | solution.py:20
  144.8 5.5 %collective-permute-start.32 = (bf16[512,768]{1,0:T(8,128)(2,1)S(1)}, bf16[512,768]{1,0:T(8,128)(2,1)S(1)}, u32[]{:S(2)}, u32[]{:S(2)}) collective-permute-start(bf16[512,768]{1,0:T(8,128)(2,1)S(1)} %get-tuple-element.12), channel_id=1, source_target_pairs={{0,1},{1,0},{2,3},{3,2},{4,5},{5,4},{6,7},{7,6},{8,9},{9,8},{10,11... | collective-permute-start | bytes 2359304 | tf_op jit(solution)/shard_map/ppermute | solution.py:20
  145.8 10.3 %collective-permute-start.29 = (bf16[128,512]{1,0:T(8,128)(2,1)S(1)}, bf16[128,512]{1,0:T(8,128)(2,1)S(1)}, u32[]{:S(2)}, u32[]{:S(2)}) collective-permute-start(bf16[128,512]{1,0:T(8,128)(2,1)S(1)} %get-tuple-element.27), channel_id=1, source_target_pairs={{0,2},{2,4},{4,6},{6,0},{1,3},{3,5},{5,7},{7,1},{8,10},{10,12},{12... | collective-permute-start | bytes 393224 | tf_op jit(solution)/shard_map/ppermute | solution.py:20
  145.9 10.3 %collective-permute-start.30 = (bf16[128,512]{1,0:T(8,128)(2,1)S(1)}, bf16[128,512]{1,0:T(8,128)(2,1)S(1)}, u32[]{:S(2)}, u32[]{:S(2)}) collective-permute-start(bf16[128,512]{1,0:T(8,128)(2,1)S(1)} %get-tuple-element.26), channel_id=1, source_target_pairs={{0,4},{2,6},{4,0},{6,2},{1,5},{3,7},{5,1},{7,3},{8,12},{10,14},{12... | collective-permute-start | bytes 393224 | tf_op jit(solution)/shard_map/ppermute | solution.py:20
  147.9 10.3 %collective-permute-start.31 = (bf16[128,512]{1,0:T(8,128)(2,1)S(1)}, bf16[128,512]{1,0:T(8,128)(2,1)S(1)}, u32[]{:S(2)}, u32[]{:S(2)}) collective-permute-start(bf16[128,512]{1,0:T(8,128)(2,1)S(1)} %get-tuple-element.25), channel_id=1, source_target_pairs={{0,6},{2,0},{4,2},{6,4},{1,7},{3,1},{5,3},{7,5},{8,14},{10,8},{12,... | collective-permute-start | bytes 393224 | tf_op jit(solution)/shard_map/ppermute | solution.py:20
  149.5 15.0 %collective-permute-start.37 = (bf16[128,768]{1,0:T(8,128)(2,1)S(1)}, bf16[128,768]{1,0:T(8,128)(2,1)S(1)}, u32[]{:S(2)}, u32[]{:S(2)}) collective-permute-start(bf16[128,768]{1,0:T(8,128)(2,1)S(1)} %get-tuple-element.19), channel_id=1, source_target_pairs={{0,2},{2,4},{4,6},{6,0},{1,3},{3,5},{5,7},{7,1},{8,10},{10,12},{12... | collective-permute-start | bytes 589832 | tf_op jit(solution)/shard_map/ppermute | solution.py:20
  150.3 19.3 %collective-permute-start.38 = (bf16[128,768]{1,0:T(8,128)(2,1)S(1)}, bf16[128,768]{1,0:T(8,128)(2,1)S(1)}, u32[]{:S(2)}, u32[]{:S(2)}) collective-permute-start(bf16[128,768]{1,0:T(8,128)(2,1)S(1)} %get-tuple-element.18), channel_id=1, source_target_pairs={{0,4},{2,6},{4,0},{6,2},{1,5},{3,7},{5,1},{7,3},{8,12},{10,14},{12... | collective-permute-start | bytes 589832 | tf_op jit(solution)/shard_map/ppermute | solution.py:20
  156.1 13.5 %collective-permute-start.39 = (bf16[128,768]{1,0:T(8,128)(2,1)S(1)}, bf16[128,768]{1,0:T(8,128)(2,1)S(1)}, u32[]{:S(2)}, u32[]{:S(2)}) collective-permute-start(bf16[128,768]{1,0:T(8,128)(2,1)S(1)} %get-tuple-element.17), channel_id=1, source_target_pairs={{0,6},{2,0},{4,2},{6,4},{1,7},{3,1},{5,3},{7,5},{8,14},{10,8},{12,... | collective-permute-start | bytes 589832 | tf_op jit(solution)/shard_map/ppermute | solution.py:20
  156.1 16.0 %collective-permute-start.33 = (bf16[128,768]{1,0:T(8,128)(2,1)S(1)}, bf16[128,768]{1,0:T(8,128)(2,1)S(1)}, u32[]{:S(2)}, u32[]{:S(2)}) collective-permute-start(bf16[128,768]{1,0:T(8,128)(2,1)S(1)} %get-tuple-element.23), channel_id=1, source_target_pairs={{0,2},{2,4},{4,6},{6,0},{1,3},{3,5},{5,7},{7,1},{8,10},{10,12},{12... | collective-permute-start | bytes 589832 | tf_op jit(solution)/shard_map/ppermute | solution.py:20
  158.1 14.0 %collective-permute-start.34 = (bf16[128,768]{1,0:T(8,128)(2,1)S(1)}, bf16[128,768]{1,0:T(8,128)(2,1)S(1)}, u32[]{:S(2)}, u32[]{:S(2)}) collective-permute-start(bf16[128,768]{1,0:T(8,128)(2,1)S(1)} %get-tuple-element.22), channel_id=1, source_target_pairs={{0,4},{2,6},{4,0},{6,2},{1,5},{3,7},{5,1},{7,3},{8,12},{10,14},{12... | collective-permute-start | bytes 589832 | tf_op jit(solution)/shard_map/ppermute | solution.py:20
  164.5 8.3 %collective-permute-start.35 = (bf16[128,768]{1,0:T(8,128)(2,1)S(1)}, bf16[128,768]{1,0:T(8,128)(2,1)S(1)}, u32[]{:S(2)}, u32[]{:S(2)}) collective-permute-start(bf16[128,768]{1,0:T(8,128)(2,1)S(1)} %get-tuple-element.21), channel_id=1, source_target_pairs={{0,6},{2,0},{4,2},{6,4},{1,7},{3,1},{5,3},{7,5},{8,14},{10,8},{12,... | collective-permute-start | bytes 589832 | tf_op jit(solution)/shard_map/ppermute | solution.py:20
